TPU v7x, 256 devices: a whole 4x4x8 slice. The times are simulated.
256 devices in a mesh: sp: 64 (over z, x, core), tp: 4 (over y).
Axes of the slice: x: 4, y: 4, z: 8, core: 2. Of those that a mesh axis runs over, the one named last changes fastest.
Arguments:
- residual: bfloat16 [8192, 2048], P(('sp', 'tp')), may hold values from -6 to 6
- query_first: bfloat16 [8192, 1024], P('sp', 'tp'), may hold values from -200 to 200
- key_first: bfloat16 [8192, 1024], P('sp', 'tp'), may hold values from -200 to 200
- query_second: bfloat16 [8192, 1024], P('sp', 'tp'), may hold values from -200 to 200
- key_second: bfloat16 [8192, 1024], P('sp', 'tp'), may hold values from -200 to 200
- values: bfloat16 [8192, 2048], P('sp', 'tp'), may hold values from -6 to 6
- lambda_weight: float32 [16], P('tp'), may hold values from 0.3 to 0.8
- head_gain: float32 [128], replicated, may hold values from 0.1 to 1.9
- out_weight: bfloat16 [2048, 2048], P('sp', 'tp'), may hold values from -0.125 to 0.125
- norm_gain: float32 [2048], replicated, may hold values from 0.1 to 1.9
- gate_weight: bfloat16 [2048, 5632], P(None, 'tp'), may hold values from -0.125 to 0.125
- up_weight: bfloat16 [2048, 5632], P(None, 'tp'), may hold values from -0.125 to 0.125
- down_weight: bfloat16 [2048, 5632], P('sp', 'tp'), may hold values from -0.078125 to 0.078125
Outputs:
- layer_out: bfloat16 [8192, 2048], P(('sp', 'tp'))
All inputs are finite; a program needn't handle non-finite values.
Results may differ from a plain program's by a relative error of at most 0.017.
Values may be sent and summed in bfloat16 or wider, within the bound.
A program may use at most 128 MiB of HBM per device.

v0:
```python
import math

import jax
import jax.numpy as jnp
from jax import lax
from jax.sharding import PartitionSpec as P

epsilon = 1e-06


def side_by_side(arrays, axis, dim, along):
    both = jnp.concatenate(arrays, axis=along)
    out, at, outs = (lax.all_gather(both, axis, axis=dim, tiled=True), 0, [])
    for a in arrays:
        outs.append(lax.slice_in_dim(out, at, at + a.shape[along], axis=along))
        at += a.shape[along]
    return tuple(outs)


def split_up(array, dim, devices):
    before, after = (array.shape[:dim], array.shape[dim + 1 :])
    return jnp.moveaxis(array.reshape(*before, devices, -1, *after), dim, 0)


def sum_at_owner(array, axis, dim):
    devices = lax.axis_size(axis)
    pieces = lax.all_to_all(split_up(array, dim, devices), axis, 0, 0, tiled=True)
    return jnp.sum(pieces.astype(jnp.float32), axis=0)


def in_order(pieces, dim):
    shape = list(pieces.shape[1:])
    shape[dim] *= pieces.shape[0]
    return jnp.moveaxis(pieces, 0, dim).reshape(shape)


def copy_for_each(array, axis):
    copies = jnp.broadcast_to(array, (lax.axis_size(axis), *array.shape))
    return lax.all_to_all(copies, axis, split_axis=0, concat_axis=0, tiled=True)


def gathered_copies(array, axis, dim):
    return in_order(copy_for_each(array, axis), dim)


def map_update(state_in, queries, key_rows, value_block, score_scale):
    maxima, totals, accumulated = state_in
    scores = (
        jnp.einsum("thd,khd->htk", queries, key_rows, preferred_element_type=jnp.float32)
        * score_scale
    )
    newest = jnp.maximum(maxima, jnp.max(scores, axis=-1))
    factor = jnp.exp(maxima - newest)
    weights = jnp.exp(scores - newest[:, :, None])
    totals = totals * factor + jnp.sum(weights, axis=-1)
    product = jnp.einsum(
        "htk,khe->the",
        weights.astype(jnp.bfloat16),
        value_block,
        preferred_element_type=jnp.float32,
    )
    accumulated = accumulated * factor.T[:, :, None] + product
    return (newest, totals, accumulated)


def local(
    residual,
    query_first,
    key_first,
    query_second,
    key_second,
    values,
    lambda_weight,
    head_gain,
    out_weight,
    norm_gain,
    gate_weight,
    up_weight,
    down_weight,
):
    tokens_here = query_first.shape[0]
    head_count = lambda_weight.shape[0]
    head_size = query_first.shape[1] // head_count
    value_size = values.shape[1] // head_count
    score_scale = head_size ** (-0.5)
    queries_first = query_first.reshape(tokens_here, head_count, head_size)
    queries_second = query_second.reshape(tokens_here, head_count, head_size)
    empty_stats = (
        jnp.full((head_count, tokens_here), -jnp.inf, jnp.float32),
        jnp.zeros((head_count, tokens_here), jnp.float32),
        jnp.zeros((tokens_here, head_count, value_size), jnp.float32),
    )
    start_state = (empty_stats, empty_stats)
    out_whole, down_whole = side_by_side((out_weight, down_weight), "sp", 0, 1)
    pieces = side_by_side((key_first, key_second, values), "sp", 0, 1)
    keys_one = pieces[0]
    row_count = keys_one.shape[0]
    block_rows = math.gcd(row_count, 1024)
    blocks = (
        keys_one.reshape(row_count // block_rows, block_rows, head_count, head_size),
        pieces[1].reshape(row_count // block_rows, block_rows, head_count, head_size),
        pieces[2].reshape(row_count // block_rows, block_rows, head_count, value_size),
    )

    def advance(current, block_keys):
        return (
            (
                map_update(current[0], queries_first, block_keys[0], block_keys[2], score_scale),
                map_update(current[1], queries_second, block_keys[1], block_keys[2], score_scale),
            ),
            None,
        )

    statistics = lax.scan(advance, start_state, blocks)[0]

    def finish(map_stats):
        return map_stats[2] / map_stats[1].T[:, :, None]

    difference = finish(statistics[0]) - lambda_weight[None, :, None] * finish(statistics[1])
    scaled = difference * lax.rsqrt(
        jnp.mean(difference * difference, axis=-1, keepdims=True) + epsilon
    )
    attended = (
        (scaled * head_gain).astype(jnp.bfloat16).reshape(tokens_here, head_count * value_size)
    )
    partial_value = lax.dot_general(
        attended, out_whole, (((1,), (1,)), ((), ())), preferred_element_type=jnp.float32
    )
    summed = sum_at_owner(partial_value.astype(jnp.bfloat16), "tp", 0)
    after_attention = (residual.astype(jnp.float32) + summed).astype(jnp.bfloat16)
    stream = after_attention.astype(jnp.float32)
    scaled_rows = stream * lax.rsqrt(jnp.mean(stream * stream, axis=-1, keepdims=True) + epsilon)
    shard_piece = gathered_copies((scaled_rows * norm_gain).astype(jnp.bfloat16), "tp", 0)
    gate_part = jnp.dot(shard_piece, gate_weight, preferred_element_type=jnp.float32)
    up_part = jnp.dot(shard_piece, up_weight, preferred_element_type=jnp.float32)
    hidden = (jax.nn.silu(gate_part) * up_part).astype(jnp.bfloat16)
    down_partial = lax.dot_general(
        hidden, down_whole, (((1,), (1,)), ((), ())), preferred_element_type=jnp.float32
    )
    feed_out = sum_at_owner(down_partial.astype(jnp.bfloat16), "tp", 0)
    return (after_attention.astype(jnp.float32) + feed_out).astype(jnp.bfloat16)


def solution(mesh):
    return jax.shard_map(
        local,
        mesh=mesh,
        in_specs=(
            P(("sp", "tp"), None),
            P("sp", "tp"),
            P("sp", "tp"),
            P("sp", "tp"),
            P("sp", "tp"),
            P("sp", "tp"),
            P("tp"),
            P(),
            P("sp", "tp"),
            P(),
            P(None, "tp"),
            P(None, "tp"),
            P("sp", "tp"),
        ),
        out_specs=P(("sp", "tp"), None),
        check_vma=False,
    )
```

profile of v0, /device:TPU:1, one launch (start us, length us, event | category | flops | bytes accessed | tf_op | source)
XLA Modules:
  0.0 339.4 jit_solution(2257808827397726490)
XLA Ops:
  6.5 1.7 pad_maximum_fusion
  11.8 101.7 %all-gather.3.cloned.1.call-done = bf16[8192,1024]{1,0:T(8,128)(2,1)} async-done(((bf16[128,1024]{1,0:T(8,128)(2,1)}), bf16[8192,1024]{1,0:T(8,128)(2,1)}) %all-gather.3.cloned.1.call-update) | async-done | bytes 16777232 | tf_op jit(solution)/shard_map/all_gather | solution.py:13
  113.5 5.7 %fusion.48 = (bf16[8192,256]{1,0:T(8,128)(2,1)}, bf16[8192,256]{1,0:T(8,128)(2,1)}) fusion(bf16[8192,1024]{1,0:T(8,128)(2,1)} %all-gather.3.cloned.1.call-done), kind=kLoop, calls=%fused_computation.74 | loop fusion | bytes 16777216 | tf_op jit(solution)/shard_map/slice | solution.py:15
  119.3 12.9 %reshape.61 = bf16[8,1024,4,64]{3,2,1,0:T(4,128)(2,1)} reshape(bf16[8192,256]{1,0:T(8,128)(2,1)} %get-tuple-element.164) | data formatting | bytes 8388608 | tf_op jit(solution)/shard_map/reshape | solution.py:100
  132.2 12.8 %copy.25 = bf16[8,1024,4,64]{1,3,2,0:T(8,128)(2,1)} copy(bf16[8,1024,4,64]{3,2,1,0:T(4,128)(2,1)} %reshape.61) | data formatting | bytes 8388608
  144.9 12.9 %reshape.63 = bf16[8,1024,4,64]{3,2,1,0:T(4,128)(2,1)} reshape(bf16[8192,256]{1,0:T(8,128)(2,1)} %get-tuple-element.163) | data formatting | bytes 8388608 | tf_op jit(solution)/shard_map/reshape | solution.py:101
  157.8 12.9 %copy.27 = bf16[8,1024,4,64]{1,3,2,0:T(8,128)(2,1)} copy(bf16[8,1024,4,64]{3,2,1,0:T(4,128)(2,1)} %reshape.63) | data formatting | bytes 8388608
  170.7 7.4 %slice.21 = bf16[8192,512]{1,0:T(8,128)(2,1)} slice(bf16[8192,1024]{1,0:T(8,128)(2,1)} %all-gather.3.cloned.1.call-done), slice={[0:8192], [512:1024]} | slice | bytes 16777216 | tf_op jit(solution)/shard_map/slice | solution.py:15
  178.0 12.6 %reshape.62 = bf16[8,1024,4,128]{3,2,1,0:T(4,128)(2,1)} reshape(bf16[8192,512]{1,0:T(8,128)(2,1)} %slice.21) | data formatting | bytes 16777216 | tf_op jit(solution)/shard_map/reshape | solution.py:102
  190.7 92.9 %while.21 = (s32[]{:T(128)}, f32[4,128]{1,0:T(4,128)S(1)}, f32[4,128]{1,0:T(4,128)}, f32[128,4,128]{0,2,1:T(8,128)S(1)}, f32[4,128]{1,0:T(4,128)S(1)}, /*index=5...) while((s32[]{:T(128)}, f32[4,128]{1,0:T(4,128)S(1)}, ...), condition=%wide.region_5.6_spmd.clone, body=%wide.region_0.5_spmd.clone.sunk | while | flops 411441152 | bytes 21202180 | solution.py:114
  192.3 2.7 constant_dynamic-slice_fusion.2
  194.9 1.6 copy.38
  197.9 1.6 bitcast_reduce_fusion.4
  201.5 1.6 bitcast_reduce_fusion.5
  203.1 2.7 constant_dynamic-slice_fusion.2
  205.7 1.6 copy.38
  207.3 2.2 fusion.82
  209.6 1.6 bitcast_reduce_fusion.4
  213.2 1.6 bitcast_reduce_fusion.5
  214.8 2.7 constant_dynamic-slice_fusion.2
  217.4 1.6 copy.38
  219.1 2.2 fusion.82
  224.9 1.6 bitcast_reduce_fusion.5
  226.5 2.7 constant_dynamic-slice_fusion.2
  229.2 1.6 copy.38
  230.8 2.2 fusion.82
  238.2 2.7 constant_dynamic-slice_fusion.2
  240.9 1.6 copy.38
  242.5 2.2 fusion.82
  244.8 1.6 bitcast_reduce_fusion.4
  248.4 1.6 bitcast_reduce_fusion.5
  250.0 2.7 constant_dynamic-slice_fusion.2
  252.6 1.6 copy.38
  254.3 2.2 fusion.82
  256.5 1.6 bitcast_reduce_fusion.4
  260.1 1.6 bitcast_reduce_fusion.5
  261.7 2.7 constant_dynamic-slice_fusion.2
  264.4 1.6 copy.38
  266.0 2.2 fusion.82
  273.4 2.7 constant_dynamic-slice_fusion.2
  276.1 1.6 copy.38
  277.7 2.2 fusion.82
  285.5 2.4 convolution_convert_fusion
  287.9 12.9 %all_to_all.15 = bf16[4,32,2048]{2,1,0:T(8,128)(2,1)S(1)} all-to-all(bf16[4,32,2048]{2,1,0:T(8,128)(2,1)S(1)} %bitcast.99), channel_id=1, replica_groups=mesh['sp'=64,'tp'=4] {'tp'}, dimensions={0} | all-to-all | bytes 1048576 | tf_op jit(solution)/shard_map/all_to_all | solution.py:27
  301.3 10.4 %all_to_all.16 = bf16[4,32,2048]{2,1,0:T(8,128)(2,1)S(1)} all-to-all(bf16[4,32,2048]{2,1,0:T(8,128)(2,1)S(1)} %broadcast_in_dim.15), channel_id=1, replica_groups=mesh['sp'=64,'tp'=4] {'tp'}, dimensions={0} | all-to-all | bytes 1048576 | tf_op jit(solution)/shard_map/all_to_all | solution.py:39
  311.6 3.6 %fusion.49 = f32[128,1408]{1,0:T(8,128)S(1)} fusion(bf16[128,2048]{1,0:T(8,128)(2,1)S(1)} %bitcast.96, bf16[2048,1408]{1,0:T(8,128)(2,1)} %param.25), kind=kOutput, calls=%fused_computation.75 | convolution fusion | flops 738197504 | bytes 7012352 | tf_op jit(solution)/shard_map/dot_general | solution.py:134
  315.3 7.2 %fusion.33 = bf16[128,2048]{1,0:T(8,128)(2,1)S(1)} fusion(bf16[2048,1920]{1,0:T(8,128)(2,1)} %all-gather.5.cloned.1.call-done, bf16[128,2048]{1,0:T(8,128)(2,1)S(1)} %bitcast.97, bf16[2048,1408]{1,0:T(8,128)(2,1)} %param.26, f32[128,1408]{1,0:T(8,128)S(1)} %fusion.49), kind=kOutput, calls=%fused_computation.47 | convolution fusion | flops 1477738496 | bytes 13303808 | tf_op jit(solution)/shard_map/dot_general | solution.py:137
  322.5 9.3 %all_to_all.17 = bf16[4,32,2048]{2,1,0:T(8,128)(2,1)S(1)} all-to-all(bf16[4,32,2048]{2,1,0:T(8,128)(2,1)S(1)} %bitcast.98), channel_id=1, replica_groups=mesh['sp'=64,'tp'=4] {'tp'}, dimensions={0} | all-to-all | bytes 1048576 | tf_op jit(solution)/shard_map/all_to_all | solution.py:27
  (164 shorter events, 34.5 us)
Async XLA Ops:
  6.5 107.0 %all-gather.3.cloned.1.call-start = ((), (), s32[]{:S(2)}) async-start(), calls=%async_computation.3 | async-start | bytes 17039360 | tf_op jit(solution)/shard_map/all_gather | solution.py:13
  8.2 277.2 %all-gather.5.cloned.1.call-start = ((), (), s32[]{:S(2)}) async-start(), calls=%async_computation.4 | async-start | bytes 7987200 | tf_op jit(solution)/shard_map/all_gather | solution.py:13
  200.1 0.7 copy-start.1
  200.1 0.7 copy-start.3
  200.9 0.6 copy-start.2
  200.9 0.6 copy-start.4
  211.8 0.7 copy-start.1
  211.8 0.7 copy-start.3
  212.6 0.6 copy-start.2
  212.6 0.6 copy-start.4
  223.5 0.7 copy-start.1
  223.6 0.7 copy-start.3
  224.3 0.6 copy-start.2
  224.3 0.6 copy-start.4
  235.3 0.7 copy-start.1
  235.3 0.7 copy-start.3
  236.1 0.6 copy-start.2
  236.1 0.6 copy-start.4
  247.0 0.7 copy-start.1
  247.0 0.7 copy-start.3
  247.8 0.6 copy-start.2
  247.8 0.6 copy-start.4
  258.7 0.7 copy-start.1
  258.7 0.7 copy-start.3
  259.5 0.6 copy-start.2
  259.5 0.6 copy-start.4
  270.5 0.7 copy-start.1
  270.5 0.7 copy-start.3
  271.2 0.6 copy-start.2
  271.3 0.6 copy-start.4
  282.2 0.7 copy-start.1
  282.2 0.7 copy-start.3
  283.0 0.6 copy-start.2
  283.0 0.6 copy-start.4
  285.4 15.5 %copy-start = (bf16[32,2048]{1,0:T(8,128)(2,1)S(1)}, bf16[32,2048]{1,0:T(8,128)(2,1)}, u32[]{:S(2)}) copy-start(bf16[32,2048]{1,0:T(8,128)(2,1)} %param.15) | copy-start | bytes 393220
  285.4 15.6 %copy-start.5 = (f32[2048]{0:T(1024)S(1)}, f32[2048]{0:T(1024)}, u32[]{:S(2)}) copy-start(f32[2048]{0:T(1024)} %param.24) | copy-start | bytes 24580
Sparse Core Ops, SparseCore 0:
  10.1 103.3 all-gather.2
  116.3 79.2 all-gather.4
where the time goes:
time: 344 us; the launch traced here: 339 us
  local copies, waits for them, and re-layouts  118 us (34%)
  waiting for transfers between devices  102 us (30%)
  matrix products  60.7 us (18%)
  blocking collectives  32.6 us (9%)
  between operations  13.5 us (4%)
  other arithmetic  12.2 us (4%)
    all_gather x2, waiting for transfers between devices, side_by_side(): out, at, outs = (lax.all_gather(both, axis, axis=dim, tiled=True), 0, [])  102 us
    dynamic_slice x16, local copies, waits for them, and re-layouts, local(): statistics = lax.scan(advance, start_state, blocks)[0]  34.1 us
    unnamed x8, local copies, waits for them, and re-layouts  27.5 us
    dot_general x16, matrix products, map_update(): jnp.einsum('thd,khd->htk', queries, key_rows, preferred_element_type=jnp....  25.3 us
    all_to_all x2, blocking collectives, sum_at_owner(): lax.all_to_all(split_up(array, dim, devices), axis, 0, 0, tiled=True)  22.3 us
    dot_general x16, matrix products, map_update(): jnp.einsum('htk,khe->the', weights.astype(jnp.bfloat16), value_block, pre...  22.1 us
    slice x2, local copies, waits for them, and re-layouts, side_by_side(): outs.append(lax.slice_in_dim(out, at, at + a.shape[along], axis=along))  13.1 us
    reshape x1, local copies, waits for them, and re-layouts, local(): keys_one.reshape(row_count // block_rows, block_rows, head_count, head_size)  12.9 us
  transfers between devices with their start and end apart: 2, of which 1 were waited for; matrix products, arithmetic and copies ran while one was open for 50% of the time, Pallas kernels for 0%

commit v1 on v0

v1 whole, which is shorter than its diff:
```python
import functools
import math

import jax
import jax.numpy as jnp
from jax import lax
from jax.experimental import pallas as pl
from jax.experimental.pallas import tpu as pltpu
from jax.sharding import PartitionSpec as P

EPS = 1e-06
MESH = pl.DeviceIdType.MESH
NX = 4
NC = 2
F32 = jnp.float32
BF16 = jnp.bfloat16


def dot_nt(a, b):
    return lax.dot_general(a, b, (((1,), (1,)), ((), ())), preferred_element_type=F32)


def attention_kernel(
    nz,
    n_tp,
    q1_ref,
    q2_ref,
    k1_ref,
    k2_ref,
    v_ref,
    lam_ref,
    gain_ref,
    att_ref,
    packq,
    packkv,
    qrecv,
    qs,
    kv,
    acc,
    mx,
    tot,
    asend,
    arecv,
    xs_sem,
    xr_sem,
    rs_sem,
    rr_sem,
    ls_sem,
    lr_sem,
    ds_sem,
    dr_sem,
    as_sem,
    ar_sem,
):
    sp = lax.axis_index("sp")
    tp = lax.axis_index("tp")
    z = sp // (NX * NC)
    x = (sp // NC) % NX
    c = sp % NC
    tokens = q1_ref.shape[0]
    rows = NX * tokens
    half = rows // 2
    steps = nz - 1

    def dev(zz, xx, cc):
        return ((zz * NX + xx) * NC + cc, tp)

    z_up = (z + 1) % nz
    z_dn = (z + nz - 1) % nz
    peers = [dev(z, (x + d) % NX, c) for d in range(1, NX)]
    peers += [dev(z_up, x, c), dev(z_dn, x, c), dev(z, x, 1 - c)]
    barrier = pltpu.get_barrier_semaphore()
    for p in peers:
        pl.semaphore_signal(barrier, inc=1, device_id=p, device_id_type=MESH)

    low = lax.broadcasted_iota(jnp.int32, (tokens, 128), 1) < 64

    def joined(first, second, j):
        a = first[:, 128 * (j // 2) : 128 * (j // 2) + 128].astype(F32)
        b = second[:, 128 * (j // 2) : 128 * (j // 2) + 128].astype(F32)
        if j % 2 == 0:
            b = pltpu.roll(b, 64, 1)
        else:
            a = pltpu.roll(a, 64, 1)
        return jnp.where(low, a, b).astype(BF16)

    for j in range(NX):
        packkv[j, 0] = joined(k1_ref, k2_ref, j)
        packkv[j, 1] = v_ref[:, 128 * j : 128 * j + 128]
        packq[j] = joined(q1_ref, q2_ref, j)
    mine = z * NC + c
    my_rows = pl.ds(pl.multiple_of(x * tokens, tokens), tokens)
    kv[mine, :, my_rows, :] = packkv[x]
    qrecv[my_rows, :] = packq[x]
    acc[...] = jnp.zeros_like(acc)
    tot[...] = jnp.zeros_like(tot)
    mx[...] = jnp.full(mx.shape, -3e38, F32)
    pl.semaphore_wait(barrier, len(peers))

    x_copies = []
    for d in range(1, NX):
        to = (x + d) % NX
        x_copies.append(
            pltpu.make_async_remote_copy(
                src_ref=packkv.at[to],
                dst_ref=kv.at[mine, :, my_rows, :],
                send_sem=xs_sem.at[d - 1],
                recv_sem=xr_sem.at[d - 1],
                device_id=dev(z, to, c),
                device_id_type=MESH,
            )
        )
    for d in range(1, NX):
        to = (x + d) % NX
        x_copies.append(
            pltpu.make_async_remote_copy(
                src_ref=packq.at[to],
                dst_ref=qrecv.at[my_rows, :],
                send_sem=xs_sem.at[NX - 1 + d - 1],
                recv_sem=xr_sem.at[NX - 1 + d - 1],
                device_id=dev(z, to, c),
                device_id_type=MESH,
            )
        )
    for copy in x_copies:
        copy.start()

    def piece(slot, which):
        off = pl.multiple_of(which * half, half)
        return kv.at[slot, :, pl.ds(off, half), :]

    def up_copy(slot, which, index):
        return pltpu.make_async_remote_copy(
            src_ref=piece(slot, which),
            dst_ref=piece(slot, which),
            send_sem=rs_sem.at[index],
            recv_sem=rr_sem.at[index],
            device_id=dev(z_up, x, c),
            device_id_type=MESH,
        )

    def down_copy(slot, which, index):
        return pltpu.make_async_remote_copy(
            src_ref=piece(slot, which),
            dst_ref=piece(slot, which),
            send_sem=ls_sem.at[index],
            recv_sem=lr_sem.at[index],
            device_id=dev(z_dn, x, c),
            device_id_type=MESH,
        )

    def side_copy(slot, which, index):
        return pltpu.make_async_remote_copy(
            src_ref=piece(slot, which),
            dst_ref=piece(slot, which),
            send_sem=ds_sem.at[index],
            recv_sem=dr_sem.at[index],
            device_id=dev(z, x, 1 - c),
            device_id_type=MESH,
        )

    def from_below(j, core):
        d = (j + 2) // 2
        which = jnp.where(j < 0, 0, (j + 2) % 2)
        return ((z + nz - d) % nz) * NC + core, which

    def from_above(j, core):
        d = (j + 2) // 2
        which = jnp.where((j < 0) | (j == steps - 1), 1, (j + 2) % 2)
        return ((z + d) % nz) * NC + core, which

    for copy in x_copies[: NX - 1]:
        copy.wait_recv()
    for h in range(2):
        up_copy(mine, h, h).start()
        down_copy(mine, h, h).start()
    for h in range(2):
        side_copy(mine, h, h).start()
    for copy in x_copies[NX - 1 :]:
        copy.wait_recv()
    lane = lax.broadcasted_iota(jnp.int32, (rows, 128), 1) < 64
    queries = qrecv[...].astype(F32)
    qs[0:rows, :] = jnp.where(lane, queries, 0.0).astype(BF16)
    qs[rows : 2 * rows, :] = jnp.where(lane, 0.0, queries).astype(BF16)

    scale = 64 ** (-0.5) * math.log2(math.e)
    tile = min(256, 2 * rows)

    def attend(blocks):
        def body(r, carry):
            at = pl.ds(pl.multiple_of(r * tile, tile), tile)
            q = qs[at, :]
            scores = []
            for slot, which in blocks:
                off = pl.multiple_of(which * half, half)
                scores.append(dot_nt(q, kv[slot, 0, pl.ds(off, half), :]))
            old = mx[at, :]
            top = None
            for s in scores:
                for lo in range(0, half, 128):
                    part = s[:, lo : lo + 128]
                    top = part if top is None else jnp.maximum(top, part)
            new = jnp.maximum(old, jnp.max(top, axis=1, keepdims=True))
            factor = jnp.exp2((old - new) * scale)
            total = tot[at, :] * factor
            product = acc[at, :] * factor
            for (slot, which), s in zip(blocks, scores):
                off = pl.multiple_of(which * half, half)
                parts = []
                for lo in range(0, half, 128):
                    part = jnp.exp2((s[:, lo : lo + 128] - new) * scale)
                    total = total + part
                    parts.append(part.astype(BF16))
                p = jnp.concatenate(parts, axis=1)
                product = product + jnp.dot(
                    p, kv[slot, 1, pl.ds(off, half), :], preferred_element_type=F32
                )
            mx[at, :] = new
            tot[at, :] = total
            acc[at, :] = product
            return carry

        lax.fori_loop(0, 2 * rows // tile, body, 0)

    attend([(mine, 0), (mine, 1)])

    def step(i, carry):
        below, below_half = from_below(i, c)
        above, above_half = from_above(i, c)
        up_copy(below, below_half, i).wait_recv()
        down_copy(above, above_half, i).wait_recv()

        @pl.when(i < steps - 2)
        def _():
            up_copy(below, below_half, i + 2).start()

        @pl.when((i < steps - 3) | (i == steps - 2))
        def _():
            down_copy(above, above_half, jnp.minimum(i + 2, steps - 1)).start()

        side_copy(below, below_half, i + 2 + 0 * below).start()
        side_copy(above, above_half, steps + i + 2).start()
        other_b, other_bh = from_below(i - 1, 1 - c)
        other_a, other_ah = from_above(i - 1, 1 - c)
        b_index = jnp.where(i == 0, 0, i + 1)
        a_index = jnp.where(i == 0, 1, steps + i + 1)
        side_copy(other_b, other_bh, b_index).wait_recv()
        side_copy(other_a, other_ah, a_index).wait_recv()
        attend([(below, below_half), (above, above_half), (other_b, other_bh), (other_a, other_ah)])
        return carry

    lax.fori_loop(0, steps, step, 0)
    other_b, other_bh = from_below(steps - 1, 1 - c)
    other_a, other_ah = from_above(steps - 1, 1 - c)
    side_copy(other_b, other_bh, steps + 1).wait_recv()
    side_copy(other_a, other_ah, 2 * steps + 1).wait_recv()
    attend([(other_b, other_bh), (other_a, other_ah)])

    weight = lam_ref[x]
    for j in range(NX):
        a, b = j * tokens, rows + j * tokens
        first = acc[a : a + tokens, :] / jnp.sum(tot[a : a + tokens, :], axis=1, keepdims=True)
        second = acc[b : b + tokens, :] / jnp.sum(tot[b : b + tokens, :], axis=1, keepdims=True)
        diff = first - weight * second
        normal = diff * lax.rsqrt(jnp.mean(diff * diff, axis=1, keepdims=True) + EPS)
        asend[j] = (normal * gain_ref[...]).astype(BF16)

    my_cols = pl.ds(pl.multiple_of(x * 128, 128), 128)
    a_copies = []
    for d in range(1, NX):
        to = (x + d) % NX
        copy = pltpu.make_async_remote_copy(
            src_ref=asend.at[to],
            dst_ref=arecv.at[:, my_cols],
            send_sem=as_sem.at[d - 1],
            recv_sem=ar_sem.at[d - 1],
            device_id=dev(z, to, c),
            device_id_type=MESH,
        )
        copy.start()
        a_copies.append(copy)
    arecv[:, my_cols] = asend[x]
    for copy in x_copies:
        copy.wait_send()
    for h in range(steps):
        up_copy(mine, 0, h).wait_send()
        down_copy(mine, 0, h).wait_send()
    for h in range(2 * steps + 2):
        side_copy(mine, 0, h).wait_send()
    for copy in a_copies:
        copy.wait()
    att_ref[...] = arecv[...]


def attention(nz, n_tp, q1, q2, k1, k2, v, lam, gain):
    tokens = q1.shape[0]
    rows = NX * tokens
    steps = nz - 1
    vmem = pl.BlockSpec(memory_space=pltpu.VMEM)
    dma = pltpu.SemaphoreType.DMA
    flops = 2 * 2 * 2 * rows * nz * NC * rows * 128
    return pl.pallas_call(
        functools.partial(attention_kernel, nz, n_tp),
        out_shape=jax.ShapeDtypeStruct((tokens, NX * 128), BF16),
        in_specs=[vmem] * 5 + [pl.BlockSpec(memory_space=pltpu.SMEM), vmem],
        out_specs=vmem,
        scratch_shapes=[
            pltpu.VMEM((NX, tokens, 128), BF16),
            pltpu.VMEM((NX, 2, tokens, 128), BF16),
            pltpu.VMEM((rows, 128), BF16),
            pltpu.VMEM((2 * rows, 128), BF16),
            pltpu.VMEM((nz * NC, 2, rows, 128), BF16),
            pltpu.VMEM((2 * rows, 128), F32),
            pltpu.VMEM((2 * rows, 128), F32),
            pltpu.VMEM((2 * rows, 128), F32),
            pltpu.VMEM((NX, tokens, 128), BF16),
            pltpu.VMEM((tokens, NX * 128), BF16),
            dma((2 * (NX - 1),)),
            dma((2 * (NX - 1),)),
            dma((steps,)),
            dma((steps,)),
            dma((steps,)),
            dma((steps,)),
            dma((2 * steps + 2,)),
            dma((2 * steps + 2,)),
            dma((NX - 1,)),
            dma((NX - 1,)),
        ],
        compiler_params=pltpu.CompilerParams(
            collective_id=0, has_side_effects=True, vmem_limit_bytes=40 * 2**20
        ),
        cost_estimate=pl.CostEstimate(flops=20 * flops, bytes_accessed=2**22, transcendentals=0),
        name="attend",
    )(q1, q2, k1, k2, v, lam, gain.reshape(1, 128))


def feed_kernel(
    n_tp,
    att_ref,
    w_ref,
    res_ref,
    gain_ref,
    gate_ref,
    up_ref,
    out_ref,
    wv,
    gv,
    uv,
    psend,
    precv,
    after,
    nsend,
    shard,
    hid,
    dsend,
    drecv,
    load_sem,
    ps_sem,
    pr_sem,
    ns_sem,
    nr_sem,
    ds_sem,
    dr_sem,
):
    sp = lax.axis_index("sp")
    tp = lax.axis_index("tp")
    loads = [
        pltpu.make_async_copy(w_ref, wv, load_sem.at[0]),
        pltpu.make_async_copy(gate_ref, gv, load_sem.at[1]),
        pltpu.make_async_copy(up_ref, uv, load_sem.at[2]),
    ]
    for load in loads:
        load.start()
    barrier = pltpu.get_barrier_semaphore()
    for d in range(1, n_tp):
        pl.semaphore_signal(
            barrier, inc=1, device_id=(sp, (tp + d) % n_tp), device_id_type=MESH
        )
    width = att_ref.shape[1]
    n_rows = res_ref.shape[0]
    features = res_ref.shape[1]
    cols = 512

    def exchange(send, recv, s_sem, r_sem):
        copies = []
        for d in range(1, n_tp):
            to = (tp + d) % n_tp
            copy = pltpu.make_async_remote_copy(
                src_ref=send.at[to],
                dst_ref=recv.at[d - 1],
                send_sem=s_sem.at[d - 1],
                recv_sem=r_sem.at[d - 1],
                device_id=(sp, to),
                device_id_type=MESH,
            )
            copy.start()
            copies.append(copy)
        return copies

    loads[0].wait()

    def project(i, carry):
        at = pl.ds(pl.multiple_of(i * cols, cols), cols)
        part = dot_nt(att_ref[...], wv[at, 0:width]).astype(BF16)
        for t in range(n_tp):
            psend[t, :, at] = part[t * n_rows : (t + 1) * n_rows, :]
        return carry

    lax.fori_loop(0, features // cols, project, 0)
    pl.semaphore_wait(barrier, n_tp - 1)
    copies = exchange(psend, precv, ps_sem, pr_sem)
    total = psend[tp].astype(F32)
    for copy in copies:
        copy.wait()
    for d in range(n_tp - 1):
        total = total + precv[d].astype(F32)
    summed = (res_ref[...].astype(F32) + total).astype(BF16)
    after[...] = summed
    stream = summed.astype(F32)
    normal = stream * lax.rsqrt(jnp.mean(stream * stream, axis=1, keepdims=True) + EPS)
    normed = (normal * gain_ref[...]).astype(BF16)
    nsend[...] = normed
    my_rows = pl.ds(pl.multiple_of(tp * n_rows, n_rows), n_rows)
    copies = []
    for d in range(1, n_tp):
        copy = pltpu.make_async_remote_copy(
            src_ref=nsend,
            dst_ref=shard.at[my_rows, :],
            send_sem=ns_sem.at[d - 1],
            recv_sem=nr_sem.at[d - 1],
            device_id=(sp, (tp + d) % n_tp),
            device_id_type=MESH,
        )
        copy.start()
        copies.append(copy)
    shard[my_rows, :] = normed
    loads[1].wait()
    loads[2].wait()
    for copy in copies:
        copy.wait()
    hidden_width = gv.shape[1]
    lo = 0
    while lo < hidden_width:
        hi = min(lo + 256, hidden_width)
        gate = jnp.dot(shard[...], gv[:, lo:hi], preferred_element_type=F32)
        up = jnp.dot(shard[...], uv[:, lo:hi], preferred_element_type=F32)
        hid[:, lo:hi] = (gate / (1.0 + jnp.exp(-gate)) * up).astype(BF16)
        lo = hi

    def down(i, carry):
        at = pl.ds(pl.multiple_of(i * cols, cols), cols)
        part = dot_nt(hid[...], wv[at, width : width + hidden_width]).astype(BF16)
        for t in range(n_tp):
            dsend[t, :, at] = part[t * n_rows : (t + 1) * n_rows, :]
        return carry

    lax.fori_loop(0, features // cols, down, 0)
    copies = exchange(dsend, drecv, ds_sem, dr_sem)
    total = dsend[tp].astype(F32)
    for copy in copies:
        copy.wait()
    for d in range(n_tp - 1):
        total = total + drecv[d].astype(F32)
    out_ref[...] = (after[...].astype(F32) + total).astype(BF16)


def feed(n_tp, att, weights, residual, gain, gate, up):
    n_rows, features = residual.shape
    tokens = att.shape[0]
    hidden = gate.shape[1]
    vmem = pl.BlockSpec(memory_space=pltpu.VMEM)
    hbm = pl.BlockSpec(memory_space=pl.ANY)
    dma = pltpu.SemaphoreType.DMA
    return pl.pallas_call(
        functools.partial(feed_kernel, n_tp),
        out_shape=jax.ShapeDtypeStruct((n_rows, features), BF16),
        in_specs=[vmem, hbm, vmem, vmem, hbm, hbm],
        out_specs=vmem,
        scratch_shapes=[
            pltpu.VMEM(weights.shape, BF16),
            pltpu.VMEM(gate.shape, BF16),
            pltpu.VMEM(up.shape, BF16),
            pltpu.VMEM((n_tp, n_rows, features), BF16),
            pltpu.VMEM((n_tp - 1, n_rows, features), BF16),
            pltpu.VMEM((n_rows, features), BF16),
            pltpu.VMEM((n_rows, features), BF16),
            pltpu.VMEM((tokens, features), BF16),
            pltpu.VMEM((tokens, hidden), BF16),
            pltpu.VMEM((n_tp, n_rows, features), BF16),
            pltpu.VMEM((n_tp - 1, n_rows, features), BF16),
            dma((3,)),
            dma((n_tp - 1,)),
            dma((n_tp - 1,)),
            dma((n_tp - 1,)),
            dma((n_tp - 1,)),
            dma((n_tp - 1,)),
            dma((n_tp - 1,)),
        ],
        compiler_params=pltpu.CompilerParams(
            collective_id=1, has_side_effects=True, vmem_limit_bytes=60 * 2**20
        ),
        name="feed",
    )(att, weights, residual, gain.reshape(1, features), gate, up)


def local(nz, n_tp, residual, q1, k1, q2, k2, v, lam, head_gain, out_w, norm_gain, gate, up, down):
    weights = lax.all_gather(jnp.concatenate([out_w, down], axis=1), "sp", axis=0, tiled=True)
    att = attention(nz, n_tp, q1, q2, k1, k2, v, lam, head_gain)
    return feed(n_tp, att, weights, residual, norm_gain, gate, up)


def solution(mesh):
    nz = mesh.shape["sp"] // (NX * NC)
    n_tp = mesh.shape["tp"]
    return jax.shard_map(
        functools.partial(local, nz, n_tp),
        mesh=mesh,
        in_specs=(
            P(("sp", "tp"), None),
            P("sp", "tp"),
            P("sp", "tp"),
            P("sp", "tp"),
            P("sp", "tp"),
            P("sp", "tp"),
            P("tp"),
            P(),
            P("sp", "tp"),
            P(),
            P(None, "tp"),
            P(None, "tp"),
            P("sp", "tp"),
        ),
        out_specs=P(("sp", "tp"), None),
        check_vma=False,
    )
```

time: 344 us -> 140 us (0.41); the launches traced: 339 us -> 139 us
  local copies, waits for them, and re-layouts: 118 us -> 7.78 us
  Pallas kernels: 0 us -> 82.9 us
  waiting for transfers between devices: 102 us -> 33.8 us
  matrix products: 60.7 us -> 0 us
  blocking collectives: 32.6 us -> 0 us
  other arithmetic: 12.2 us -> 1.55 us
    pallas_call x0 -> x2, Pallas kernels: none -> 82.9 us  [the longest x1 49.1 us: attention(): pl.pallas_call(functools.partial(attention_kernel, nz, n_tp), out_shape=j...]
    all_gather x2 -> x1, waiting for transfers between devices: 102 us -> 33.8 us  [local(): lax.all_gather(jnp.concatenate([out_w, down], axis=1), 'sp', axis=0, tile...]
    dot_general x35 -> x0, matrix products: 60.7 us -> none  [the longest x16 25.3 us: map_update(): jnp.einsum('thd,khd->htk', queries, key_rows, preferred_element_type=jnp....]
    reshape x3 -> x0, local copies, waits for them, and re-layouts: 38.4 us -> none  [the longest x1 12.9 us: local(): keys_one.reshape(row_count // block_rows, block_rows, head_count, head_size)]
    dynamic_slice x16 -> x0, local copies, waits for them, and re-layouts: 34.1 us -> none  [local(): statistics = lax.scan(advance, start_state, blocks)[0]]
    all_to_all x3 -> x0, blocking collectives: 32.6 us -> none  [the longest x2 22.3 us: sum_at_owner(): lax.all_to_all(split_up(array, dim, devices), axis, 0, 0, tiled=True)]
    unnamed x8 -> x17, local copies, waits for them, and re-layouts: 27.5 us -> 7.78 us
    slice x2 -> x0, local copies, waits for them, and re-layouts: 13.1 us -> none  [side_by_side(): outs.append(lax.slice_in_dim(out, at, at + a.shape[along], axis=along))]
  transfers between devices with their start and end apart: 2 -> 1, of which waited for: 1 -> 1; matrix products, arithmetic and copies ran while one was open for 50% -> 0% of each run, Pallas kernels for 0% -> 35%
where the time goes in v1:
time: 140 us; the launch traced here: 139 us
  Pallas kernels  82.9 us (59%)
  waiting for transfers between devices  33.8 us (24%)
  between operations  13.4 us (10%)
  local copies, waits for them, and re-layouts  7.78 us (6%)
  other arithmetic  1.55 us (1%)
    pallas_call x1, Pallas kernels, attention(): pl.pallas_call(functools.partial(attention_kernel, nz, n_tp), out_shape=j...  49.1 us
    all_gather x1, waiting for transfers between devices, local(): lax.all_gather(jnp.concatenate([out_w, down], axis=1), 'sp', axis=0, tile...  33.8 us
    pallas_call x1, Pallas kernels, feed(): pl.pallas_call(functools.partial(feed_kernel, n_tp), out_shape=jax.ShapeD...  33.7 us
    unnamed x17, local copies, waits for them, and re-layouts  7.78 us
  transfers between devices with their start and end apart: 1, of which 1 were waited for; matrix products, arithmetic and copies ran while one was open for 0% of the time, Pallas kernels for 35%

profile of v1, /device:TPU:1, one launch (start us, length us, event | category | flops | bytes accessed | tf_op | source)
XLA Modules:
  0.0 139.4 jit_solution(5200851645269535865)
XLA Ops:
  6.5 0.0 all-gather.2.cloned.1.call-start
  6.5 1.5 %pad_maximum_fusion = bf16[32,1920]{1,0:T(8,128)(2,1)} fusion(bf16[32,1408]{1,0:T(8,128)(2,1)} %param.25, bf16[32,512]{1,0:T(8,128)(2,1)} %param.21), kind=kLoop, calls=%fused_computation | loop fusion | flops 245760 | bytes 245760 | tf_op jit(solution)/shard_map/concatenate | solution.py:507
  8.1 0.0 all-gather.2.cloned.1.call-update
  8.1 0.0 copy-start.1
  8.1 0.9 copy-done.1
  9.0 0.0 copy-start.2
  9.0 0.8 copy-done.2
  9.9 0.0 copy-start.3
  9.9 0.8 copy-done.3
  10.7 0.0 copy-start.4
  10.7 0.8 copy-done.4
  11.5 0.0 copy-start.5
  11.5 0.8 copy-done.5
  12.4 0.0 copy-start.6
  12.4 0.7 copy-done.6
  13.0 0.0 copy-start.7
  13.0 0.7 copy-done.7
  13.7 49.1 %attend.1.att_ref = bf16[128,512]{1,0:T(8,128)(2,1)S(1)} custom-call(bf16[128,256]{1,0:T(8,128)(2,1)S(1)} %copy-done.2, bf16[128,256]{1,0:T(8,128)(2,1)S(1)} %copy-done.3, bf16[128,256]{1,0:T(8,128)(2,1)S(1)} %copy-done.4, bf16[128,256]{1,0:T(8,128)(2,1)S(1)} %copy-done.5, bf16[128,512]{1,0:T(8,128)(2,1)S(1)} %copy-done.1, f32[4]{0:T(128)S(1)} %copy-done.6, ...), custom_call_target="tpu_custom_call" | custom-call | flops 85899345920 | bytes 4194304 | tf_op jit(solution)/shard_map/attend/pallas_call | solution.py:302
  62.8 0.0 copy-start
  62.9 0.6 copy-done
  63.5 33.8 %all-gather.2.cloned.1.call-done.w_ref = bf16[2048,1920]{1,0:T(8,128)(2,1)} async-done(((bf16[32,1920]{1,0:T(8,128)(2,1)}), bf16[2048,1920]{1,0:T(8,128)(2,1)}) %all-gather.2.cloned.1.call-update) | async-done | bytes 7864336 | tf_op jit(solution)/shard_map/all_gather | solution.py:507
  97.3 33.7 %feed.1 = bf16[32,2048]{1,0:T(8,128)(2,1)} custom-call(bf16[128,512]{1,0:T(8,128)(2,1)} %copy-done, bf16[2048,1920]{1,0:T(8,128)(2,1)} %all-gather.2.cloned.1.call-done.w_ref, bf16[32,2048]{1,0:T(8,128)(2,1)} %res_ref.1, f32[1,2048]{1,0:T(1,128)} %bitcast.3, bf16[2048,1408]{1,0:T(8,128)(2,1)} %gate_ref.1, bf16[2048,1408]{1,0:T(8,128)(2,1)} %up_ref.1), custom_call_target="tpu_custom_call" | custom-call | tf_op jit(solution)/shard_map/feed/pallas_call | solution.py:474
  131.0 1.6 %copy.15 = bf16[32,2048]{1,0:T(8,128)(2,1)} copy(bf16[32,2048]{1,0:T(8,128)(2,1)} %feed.1) | data formatting | bytes 262144
Async XLA Ops:
  6.5 90.8 %all-gather.2.cloned.1.call-start = ((), (), s32[]{:S(2)}) async-start(), calls=%async_computation | async-start | bytes 7987200 | tf_op jit(solution)/shard_map/all_gather | solution.py:507
  8.1 0.9 copy-start.1
  9.0 0.8 copy-start.2
  9.9 0.8 copy-start.3
  10.7 0.8 copy-start.4
  11.5 0.8 copy-start.5
  12.4 0.7 copy-start.6
  13.0 0.7 copy-start.7
  62.8 0.7 copy-start
Sparse Core Ops, SparseCore 0:
  10.1 87.1 all-gather.1

commit v2 on v0

v2 whole, which is shorter than its diff:
```python
import functools
import math

import jax
import jax.numpy as jnp
from jax import lax
from jax.experimental import pallas as pl
from jax.experimental.pallas import tpu as pltpu
from jax.sharding import PartitionSpec as P

EPS = 1e-06
MESH = pl.DeviceIdType.MESH
NX = 4
NC = 2
DOWN_AT = 4
F32 = jnp.float32
BF16 = jnp.bfloat16


def dot_nt(a, b):
    return lax.dot_general(a, b, (((1,), (1,)), ((), ())), preferred_element_type=F32)


def remote(src, dst, send, recv, device):
    return pltpu.make_async_remote_copy(
        src_ref=src,
        dst_ref=dst,
        send_sem=send,
        recv_sem=recv,
        device_id=device,
        device_id_type=MESH,
    )


def kernel(
    nz,
    n_tp,
    res_hbm,
    q1_hbm,
    k1_hbm,
    q2_hbm,
    k2_hbm,
    v_hbm,
    lam_ref,
    hgain_ref,
    outw_hbm,
    ngain_ref,
    gate_hbm,
    up_hbm,
    downw_hbm,
    out_ref,
    res,
    q1,
    k1,
    q2,
    k2,
    v,
    gv,
    uv,
    wo,
    wd,
    packq,
    packkv,
    qrecv,
    qs,
    kv,
    acc,
    mx,
    tot,
    asend,
    arecv,
    psend,
    precv,
    after,
    nsend,
    shard,
    hid,
    dsend,
    drecv,
    load_sem,
    xs_sem,
    xr_sem,
    us_sem,
    ur_sem,
    ls_sem,
    lr_sem,
    ds_sem,
    dr_sem,
    as_sem,
    ar_sem,
    wus_sem,
    wur_sem,
    wls_sem,
    wlr_sem,
    wxs_sem,
    wxr_sem,
    wds_sem,
    wdr_sem,
    ps_sem,
    pr_sem,
    ns_sem,
    nr_sem,
    fs_sem,
    fr_sem,
):
    sp = lax.axis_index("sp")
    tp = lax.axis_index("tp")
    z = sp // (NX * NC)
    x = (sp // NC) % NX
    c = sp % NC
    tokens = q1.shape[0]
    rows = NX * tokens
    steps = NX * (nz - 1) // 2
    mid = nz // 2
    half = NX // 2

    def dev(zz, xx, cc):
        return ((zz * NX + xx) * NC + cc, tp)

    z_up = (z + 1) % nz
    z_dn = (z + nz - 1) % nz
    other = dev(z, x, 1 - c)

    loads = []
    for n, (src, dst) in enumerate(
        (
            (k1_hbm, k1),
            (k2_hbm, k2),
            (v_hbm, v),
            (q1_hbm, q1),
            (q2_hbm, q2),
            (outw_hbm, wo.at[z, x, c]),
            (downw_hbm, wd.at[z, x, c]),
            (gate_hbm, gv),
            (up_hbm, uv),
            (res_hbm, res),
        )
    ):
        load = pltpu.make_async_copy(src, dst, load_sem.at[n])
        load.start()
        loads.append(load)

    peers = [dev(z, (x + d) % NX, c) for d in range(1, NX)]
    peers += [dev(z_up, x, c), dev(z_dn, x, c), other]
    peers += [(sp, (tp + d) % n_tp) for d in range(1, n_tp)]
    barrier = pltpu.get_barrier_semaphore()
    for p in peers:
        pl.semaphore_signal(barrier, inc=1, device_id=p, device_id_type=MESH)

    low = lax.broadcasted_iota(jnp.int32, (tokens, 128), 1) < 64

    def joined(first, second, j):
        a = first[:, 128 * (j // 2) : 128 * (j // 2) + 128].astype(F32)
        b = second[:, 128 * (j // 2) : 128 * (j // 2) + 128].astype(F32)
        if j % 2 == 0:
            b = pltpu.roll(b, 64, 1)
        else:
            a = pltpu.roll(a, 64, 1)
        return jnp.where(low, a, b).astype(BF16)

    mine = z * NC + c
    my_rows = pl.ds(pl.multiple_of(x * tokens, tokens), tokens)
    for load in loads[:3]:
        load.wait()
    for j in range(NX):
        packkv[j, 0] = joined(k1, k2, j)
        packkv[j, 1] = v[:, 128 * j : 128 * j + 128]
    kv[mine, :, my_rows, :] = packkv[x]
    for load in loads[3:5]:
        load.wait()
    for j in range(NX):
        packq[j] = joined(q1, q2, j)
    qrecv[my_rows, :] = packq[x]
    pl.semaphore_wait(barrier, len(peers))

    order = [0, 1, NX - 1] + list(range(2, NX - 1))

    def source(s):
        back = s
        for n, d in enumerate(order):
            back = jnp.where(s == n, d, back)
        return (x + NX - back) % NX

    def piece(slot, s):
        at = pl.multiple_of(source(s) * tokens, tokens)
        return kv.at[slot, :, pl.ds(at, tokens), :]

    def up_copy(slot, s, index):
        part = piece(slot, s)
        return remote(part, part, us_sem.at[index], ur_sem.at[index], dev(z_up, x, c))

    def low_copy(slot, s, index):
        part = piece(slot, s)
        return remote(part, part, ls_sem.at[index], lr_sem.at[index], dev(z_dn, x, c))

    def side_copy(slot, s, index):
        part = piece(slot, s)
        return remote(part, part, ds_sem.at[index], dr_sem.at[index], other)

    def from_below(j, core):
        d = (j + NX) // NX
        s = jnp.where(j < 0, 2 * (j + half), (j + NX) % NX)
        return ((z + nz - d) % nz) * NC + core, s

    def from_above(j, core):
        d = (j + NX) // NX
        s = (j + NX) % NX
        s = jnp.where(j < 0, 2 * (j + half) + 1, jnp.where(j >= steps - half, s + half, s))
        return ((z + d) % nz) * NC + core, s

    up_copy(mine, 0, 0).start()
    low_copy(mine, 0, 0).start()
    side_copy(mine, 0, 0).start()
    x_copies = {}
    for d in order[1:]:
        to = (x + d) % NX
        x_copies[d] = remote(
            packkv.at[to],
            kv.at[mine, :, my_rows, :],
            xs_sem.at[d - 1],
            xr_sem.at[d - 1],
            dev(z, to, c),
        )
        x_copies[d].start()
    q_copies = []
    for d in order[1:]:
        to = (x + d) % NX
        copy = remote(
            packq.at[to],
            qrecv.at[my_rows, :],
            xs_sem.at[NX + d - 2],
            xr_sem.at[NX + d - 2],
            dev(z, to, c),
        )
        copy.start()
        q_copies.append(copy)
    for s, d in enumerate(order[1:], 1):
        x_copies[d].wait_recv()
        up_copy(mine, s, s).start()
        low_copy(mine, s, s).start()
        side_copy(mine, s, s).start()

    class Weight:
        def __init__(self, ref, n):
            self.ref = ref
            self.n = n

        def up(self, zz, k):
            block = self.ref.at[zz, x, c]
            at = self.n * mid + k - 1
            return remote(block, block, wus_sem.at[at], wur_sem.at[at], dev(z_up, x, c))

        def low(self, zz, k):
            block = self.ref.at[zz, x, c]
            at = self.n * mid + k - 1
            return remote(block, block, wls_sem.at[at], wlr_sem.at[at], dev(z_dn, x, c))

        def across(self, zz, d):
            block = self.ref.at[zz, x, c]
            at = (self.n * (NX - 1) + d - 1) * nz + zz
            return remote(block, block, wxs_sem.at[at], wxr_sem.at[at], dev(z, (x + d) % NX, c))

        def side(self, d):
            block = self.ref.at[:, (x + NX - d) % NX, c]
            at = self.n * NX + d
            return remote(block, block, wds_sem.at[at], wdr_sem.at[at], other)

        def begin(self):
            self.up(z, 1).start()
            self.low(z, 1).start()
            for d in order[1:]:
                self.across(z, d).start()

        def relay(self, k):
            below = (z + nz - k) % nz
            above = (z + k) % nz

            @pl.when((k < mid) | (c == 0))
            def _():
                self.up(below, k).wait_recv()

            @pl.when((k < mid) | (c == 1))
            def _():
                self.low(above, k).wait_recv()

            @pl.when((k < mid - 1) | ((k == mid - 1) & (c == 0)))
            def _():
                self.up(below, k + 1).start()

            @pl.when((k < mid - 1) | ((k == mid - 1) & (c == 1)))
            def _():
                self.low(above, k + 1).start()

            for d in order[1:]:
                self.across(below, d).start()

            @pl.when(k < mid)
            def _():
                for d in order[1:]:
                    self.across(above, d).start()

        def gather_side(self, d):
            if d:
                for zz in range(nz):
                    self.across(zz, d).wait_recv()
            self.side(d).start()

        def finish_side(self):
            for d in range(NX):
                self.side(d).wait_recv()

        def finish_sends(self):
            for k in range(1, mid):
                self.up(z, k).wait_send()
                self.low(z, k).wait_send()

            @pl.when(c == 0)
            def _():
                self.up(z, mid).wait_send()

            @pl.when(c == 1)
            def _():
                self.low(z, mid).wait_send()

            for d in range(1, NX):
                for zz in range(nz):
                    self.across(zz, d).wait_send()
            for d in range(NX):
                self.side(d).wait_send()

    w_out = Weight(wo, 0)
    w_down = Weight(wd, 1)
    loads[5].wait()
    w_out.begin()

    acc[...] = jnp.zeros_like(acc)
    tot[...] = jnp.zeros_like(tot)
    mx[...] = jnp.full(mx.shape, -3e38, F32)
    for copy in q_copies:
        copy.wait_recv()
    lane = lax.broadcasted_iota(jnp.int32, (rows, 128), 1) < 64
    queries = qrecv[...].astype(F32)
    qs[0:rows, :] = jnp.where(lane, queries, 0.0).astype(BF16)
    qs[rows : 2 * rows, :] = jnp.where(lane, 0.0, queries).astype(BF16)
    loads[6].wait()

    scale = 64 ** (-0.5) * math.log2(math.e)
    tile = min(256, 2 * rows)

    def attend(blocks):
        width = len(blocks) * tokens

        def body(r, carry):
            at = pl.ds(pl.multiple_of(r * tile, tile), tile)
            keys = jnp.concatenate([piece(slot, s)[0] for slot, s in blocks], axis=0)
            vals = jnp.concatenate([piece(slot, s)[1] for slot, s in blocks], axis=0)
            scores = dot_nt(qs[at, :], keys)
            old = mx[at, :]
            top = scores[:, 0:128]
            for lo in range(128, width, 128):
                top = jnp.maximum(top, scores[:, lo : lo + 128])
            new = jnp.maximum(old, jnp.max(top, axis=1, keepdims=True))
            factor = jnp.exp2((old - new) * scale)
            total = tot[at, :] * factor
            parts = []
            for lo in range(0, width, 128):
                part = jnp.exp2((scores[:, lo : lo + 128] - new) * scale)
                total = total + part
                parts.append(part.astype(BF16))
            mx[at, :] = new
            tot[at, :] = total
            acc[at, :] = acc[at, :] * factor + jnp.dot(
                jnp.concatenate(parts, axis=1), vals, preferred_element_type=F32
            )
            return carry

        lax.fori_loop(0, 2 * rows // tile, body, 0)

    attend([(mine, s) for s in range(NX)])

    def step(i, carry):
        below, below_s = from_below(i, c)
        above, above_s = from_above(i, c)
        up_copy(below, below_s, i).wait_recv()

        @pl.when(i < steps - NX)
        def _():
            up_copy(below, below_s, i + NX).start()

        low_copy(above, above_s, i).wait_recv()

        @pl.when((i < steps - NX - half) | ((i >= steps - NX) & (i < steps - half)))
        def _():
            to = jnp.where(i < steps - NX - half, i + NX, i + half)
            low_copy(above, above_s, to).start()

        side_copy(below, below_s, NX + i).start()
        side_copy(above, above_s, NX + steps + i).start()

        @pl.when((i % 2 == 1) & (i < 2 * mid))
        def _():
            w_out.relay((i + 1) // 2)

        @pl.when(i == DOWN_AT)
        def _():
            w_down.begin()

        @pl.when((i % 2 == 0) & (i > DOWN_AT) & (i <= DOWN_AT + 2 * mid))
        def _():
            w_down.relay((i - DOWN_AT) // 2)

        other_b, other_bs = from_below(i - half, 1 - c)
        other_a, other_as = from_above(i - half, 1 - c)
        b_index = jnp.where(i < half, 2 * i, NX + i - half)
        a_index = jnp.where(i < half, 2 * i + 1, NX + steps + i - half)
        side_copy(other_b, other_bs, b_index).wait_recv()
        side_copy(other_a, other_as, a_index).wait_recv()
        attend([(below, below_s), (above, above_s), (other_b, other_bs), (other_a, other_as)])
        return carry

    lax.fori_loop(0, steps, step, 0)
    w_out.gather_side(0)
    last = []
    for j in range(steps - half, steps):
        b = from_below(j, 1 - c)
        a = from_above(j, 1 - c)
        side_copy(*b, NX + j).wait_recv()
        side_copy(*a, NX + steps + j).wait_recv()
        last += [b, a]
    for d in order[1:]:
        w_out.gather_side(d)
    attend(last)

    weight = lam_ref[x]
    for j in range(NX):
        a, b = j * tokens, rows + j * tokens
        first = acc[a : a + tokens, :] / jnp.sum(tot[a : a + tokens, :], axis=1, keepdims=True)
        second = acc[b : b + tokens, :] / jnp.sum(tot[b : b + tokens, :], axis=1, keepdims=True)
        diff = first - weight * second
        normal = diff * lax.rsqrt(jnp.mean(diff * diff, axis=1, keepdims=True) + EPS)
        asend[j] = (normal * hgain_ref[...]).astype(BF16)

    my_cols = pl.ds(pl.multiple_of(x * 128, 128), 128)
    a_copies = []
    for d in order[1:]:
        to = (x + d) % NX
        copy = remote(
            asend.at[to],
            arecv.at[:, my_cols],
            as_sem.at[d - 1],
            ar_sem.at[d - 1],
            dev(z, to, c),
        )
        copy.start()
        a_copies.append(copy)
    arecv[:, my_cols] = asend[x]
    w_out.finish_side()
    for copy in a_copies:
        copy.wait()

    n_rows = res.shape[0]
    width = wo.shape[4]
    hidden_width = wd.shape[4]
    feature_rows = NX * NC * wo.shape[3]

    def exchange(send, recv, s_sem, r_sem):
        copies = []
        for d in range(1, n_tp):
            to = (tp + d) % n_tp
            copy = remote(send.at[to], recv.at[d - 1], s_sem.at[d - 1], r_sem.at[d - 1], (sp, to))
            copy.start()
            copies.append(copy)
        return copies

    def project(i, carry):
        at = pl.ds(pl.multiple_of(i * feature_rows, feature_rows), feature_rows)
        part = dot_nt(arecv[...], wo[i].reshape(feature_rows, width)).astype(BF16)
        for t in range(n_tp):
            psend[t, :, at] = part[t * n_rows : (t + 1) * n_rows, :]
        return carry

    lax.fori_loop(0, nz, project, 0)
    copies = exchange(psend, precv, ps_sem, pr_sem)
    loads[9].wait()
    total = psend[tp].astype(F32)
    for copy in copies:
        copy.wait()
    for d in range(n_tp - 1):
        total = total + precv[d].astype(F32)
    summed = (res[...].astype(F32) + total).astype(BF16)
    after[...] = summed
    stream = summed.astype(F32)
    normal = stream * lax.rsqrt(jnp.mean(stream * stream, axis=1, keepdims=True) + EPS)
    normed = (normal * ngain_ref[...]).astype(BF16)
    nsend[...] = normed
    my_part = pl.ds(pl.multiple_of(tp * n_rows, n_rows), n_rows)
    copies = []
    for d in range(1, n_tp):
        copy = remote(
            nsend,
            shard.at[my_part, :],
            ns_sem.at[d - 1],
            nr_sem.at[d - 1],
            (sp, (tp + d) % n_tp),
        )
        copy.start()
        copies.append(copy)
    shard[my_part, :] = normed
    w_down.gather_side(0)
    loads[7].wait()
    loads[8].wait()
    for copy in copies:
        copy.wait()
    lo = 0
    while lo < hidden_width:
        hi = min(lo + 256, hidden_width)
        gate = jnp.dot(shard[...], gv[:, lo:hi], preferred_element_type=F32)
        up = jnp.dot(shard[...], uv[:, lo:hi], preferred_element_type=F32)
        hid[:, lo:hi] = (gate / (1.0 + jnp.exp(-gate)) * up).astype(BF16)
        lo = hi
    for d in order[1:]:
        w_down.gather_side(d)
    w_down.finish_side()

    def down(i, carry):
        at = pl.ds(pl.multiple_of(i * feature_rows, feature_rows), feature_rows)
        part = dot_nt(hid[...], wd[i].reshape(feature_rows, hidden_width)).astype(BF16)
        for t in range(n_tp):
            dsend[t, :, at] = part[t * n_rows : (t + 1) * n_rows, :]
        return carry

    lax.fori_loop(0, nz, down, 0)
    copies = exchange(dsend, drecv, fs_sem, fr_sem)

    for d in range(1, NX):
        x_copies[d].wait_send()
    for copy in q_copies:
        copy.wait_send()
    for n in range(steps):
        up_copy(mine, 0, n).wait_send()
        low_copy(mine, 0, n).wait_send()
    for n in range(NX + 2 * steps):
        side_copy(mine, 0, n).wait_send()
    w_out.finish_sends()
    w_down.finish_sends()

    total = dsend[tp].astype(F32)
    for copy in copies:
        copy.wait()
    for d in range(n_tp - 1):
        total = total + drecv[d].astype(F32)
    out_ref[...] = (after[...].astype(F32) + total).astype(BF16)


def local(nz, n_tp, residual, q1, k1, q2, k2, v, lam, head_gain, out_w, norm_gain, gate, up, down):
    tokens = q1.shape[0]
    rows = NX * tokens
    n_rows, features = residual.shape
    hidden = gate.shape[1]
    steps = NX * (nz - 1) // 2
    mid = nz // 2
    vmem = pl.BlockSpec(memory_space=pltpu.VMEM)
    smem = pl.BlockSpec(memory_space=pltpu.SMEM)
    hbm = pl.BlockSpec(memory_space=pl.ANY)
    dma = pltpu.SemaphoreType.DMA

    def like(a):
        return pltpu.VMEM(a.shape, a.dtype)

    return pl.pallas_call(
        functools.partial(kernel, nz, n_tp),
        out_shape=jax.ShapeDtypeStruct((n_rows, features), BF16),
        in_specs=[hbm] * 6 + [smem, vmem, hbm, vmem, hbm, hbm, hbm],
        out_specs=vmem,
        scratch_shapes=[
            like(residual),
            like(q1),
            like(k1),
            like(q2),
            like(k2),
            like(v),
            like(gate),
            like(up),
            pltpu.VMEM((nz, NX, NC, *out_w.shape), BF16),
            pltpu.VMEM((nz, NX, NC, *down.shape), BF16),
            pltpu.VMEM((NX, tokens, 128), BF16),
            pltpu.VMEM((NX, 2, tokens, 128), BF16),
            pltpu.VMEM((rows, 128), BF16),
            pltpu.VMEM((2 * rows, 128), BF16),
            pltpu.VMEM((nz * NC, 2, rows, 128), BF16),
            pltpu.VMEM((2 * rows, 128), F32),
            pltpu.VMEM((2 * rows, 128), F32),
            pltpu.VMEM((2 * rows, 128), F32),
            pltpu.VMEM((NX, tokens, 128), BF16),
            pltpu.VMEM((tokens, NX * 128), BF16),
            pltpu.VMEM((n_tp, n_rows, features), BF16),
            pltpu.VMEM((n_tp - 1, n_rows, features), BF16),
            pltpu.VMEM((n_rows, features), BF16),
            pltpu.VMEM((n_rows, features), BF16),
            pltpu.VMEM((tokens, features), BF16),
            pltpu.VMEM((tokens, hidden), BF16),
            pltpu.VMEM((n_tp, n_rows, features), BF16),
            pltpu.VMEM((n_tp - 1, n_rows, features), BF16),
            dma((10,)),
            dma((2 * (NX - 1),)),
            dma((2 * (NX - 1),)),
            dma((steps,)),
            dma((steps,)),
            dma((steps,)),
            dma((steps,)),
            dma((NX + 2 * steps,)),
            dma((NX + 2 * steps,)),
            dma((NX - 1,)),
            dma((NX - 1,)),
            dma((2 * mid,)),
            dma((2 * mid,)),
            dma((2 * mid,)),
            dma((2 * mid,)),
            dma((2 * (NX - 1) * nz,)),
            dma((2 * (NX - 1) * nz,)),
            dma((2 * NX,)),
            dma((2 * NX,)),
            dma((n_tp - 1,)),
            dma((n_tp - 1,)),
            dma((n_tp - 1,)),
            dma((n_tp - 1,)),
            dma((n_tp - 1,)),
            dma((n_tp - 1,)),
        ],
        compiler_params=pltpu.CompilerParams(
            collective_id=0, has_side_effects=True, vmem_limit_bytes=62 * 2**20
        ),
        name="layer",
    )(
        residual,
        q1,
        k1,
        q2,
        k2,
        v,
        lam,
        head_gain.reshape(1, 128),
        out_w,
        norm_gain.reshape(1, features),
        gate,
        up,
        down,
    )


def solution(mesh):
    nz = mesh.shape["sp"] // (NX * NC)
    n_tp = mesh.shape["tp"]
    return jax.shard_map(
        functools.partial(local, nz, n_tp),
        mesh=mesh,
        in_specs=(
            P(("sp", "tp"), None),
            P("sp", "tp"),
            P("sp", "tp"),
            P("sp", "tp"),
            P("sp", "tp"),
            P("sp", "tp"),
            P("tp"),
            P(),
            P("sp", "tp"),
            P(),
            P(None, "tp"),
            P(None, "tp"),
            P("sp", "tp"),
        ),
        out_specs=P(("sp", "tp"), None),
        check_vma=False,
    )
```

time: 344 us -> 101 us (0.29); the launches traced: 339 us -> 101 us
  local copies, waits for them, and re-layouts: 118 us -> 1.57 us
  waiting for transfers between devices: 102 us -> 0 us
  Pallas kernels: 0 us -> 99.2 us
  matrix products: 60.7 us -> 0 us
  blocking collectives: 32.6 us -> 0 us
  between operations: 13.5 us -> 0.01 us
  other arithmetic: 12.2 us -> 0 us
    all_gather x2 -> x0, waiting for transfers between devices: 102 us -> none  [side_by_side(): out, at, outs = (lax.all_gather(both, axis, axis=dim, tiled=True), 0, [])]
    pallas_call x0 -> x1, Pallas kernels: none -> 99.2 us  [local(): pl.pallas_call(functools.partial(kernel, nz, n_tp), out_shape=jax.ShapeDt...]
    dot_general x35 -> x0, matrix products: 60.7 us -> none  [the longest x16 25.3 us: map_update(): jnp.einsum('thd,khd->htk', queries, key_rows, preferred_element_type=jnp....]
    reshape x3 -> x0, local copies, waits for them, and re-layouts: 38.4 us -> none  [the longest x1 12.9 us: local(): keys_one.reshape(row_count // block_rows, block_rows, head_count, head_size)]
    dynamic_slice x16 -> x0, local copies, waits for them, and re-layouts: 34.1 us -> none  [local(): statistics = lax.scan(advance, start_state, blocks)[0]]
    all_to_all x3 -> x0, blocking collectives: 32.6 us -> none  [the longest x2 22.3 us: sum_at_owner(): lax.all_to_all(split_up(array, dim, devices), axis, 0, 0, tiled=True)]
    unnamed x8 -> x1, local copies, waits for them, and re-layouts: 27.5 us -> 1.57 us
    slice x2 -> x0, local copies, waits for them, and re-layouts: 13.1 us -> none  [side_by_side(): outs.append(lax.slice_in_dim(out, at, at + a.shape[along], axis=along))]
  transfers between devices with their start and end apart: 2 -> 0, of which waited for: 1 -> 0; matrix products, arithmetic and copies ran while one was open for 50% -> 0% of each run, Pallas kernels for 0% -> 0%
where the time goes in v2:
time: 101 us
  Pallas kernels  99.2 us (98%)
  local copies, waits for them, and re-layouts  1.57 us (2%)
    pallas_call x1, Pallas kernels, local(): pl.pallas_call(functools.partial(kernel, nz, n_tp), out_shape=jax.ShapeDt...  99.2 us

profile of v2, /device:TPU:1, one launch (start us, length us, event | category | flops | bytes accessed | tf_op | source)
XLA Modules:
  0.0 100.7 jit_solution(16705607274397157673)
XLA Ops:
  0.0 99.2 %layer.1 = bf16[32,2048]{1,0:T(8,128)(2,1)} custom-call(bf16[32,2048]{1,0:T(8,128)(2,1)} %res_hbm.1, bf16[128,256]{1,0:T(8,128)(2,1)} %q1_hbm.1, bf16[128,256]{1,0:T(8,128)(2,1)} %k1_hbm.1, bf16[128,256]{1,0:T(8,128)(2,1)} %q2_hbm.1, bf16[128,256]{1,0:T(8,128)(2,1)} %k2_hbm.1, bf16[128,512]{1,0:T(8,128)(2,1)} %v_hbm.1, f32[4]{0:T(128)} %lam_ref.1, ...), custom_call_target="tpu_custom_call" | custom-call | tf_op jit(solution)/shard_map/layer/pallas_call | solution.py:570
  99.2 1.6 %copy.15 = bf16[32,2048]{1,0:T(8,128)(2,1)} copy(bf16[32,2048]{1,0:T(8,128)(2,1)} %layer.1) | data formatting | bytes 262144

commit v3 on v2

--- a/solution.py
+++ b/solution.py
@@ -13,6 +13,11 @@
 NX = 4
 NC = 2
 DOWN_AT = 4
+EARLY = 2
+OUT_ON = 5
+DOWN_ON = 10
+DOWN_N = 2
+PARTS = 4
 F32 = jnp.float32
 BF16 = jnp.bfloat16
 
@@ -74,6 +79,8 @@
     after,
     nsend,
     shard,
+    gacc,
+    uacc,
     hid,
     dsend,
     drecv,
@@ -241,9 +248,10 @@
         side_copy(mine, s, s).start()
 
     class Weight:
-        def __init__(self, ref, n):
+        def __init__(self, ref, n, early):
             self.ref = ref
             self.n = n
+            self.early = early
 
         def up(self, zz, k):
             block = self.ref.at[zz, x, c]
@@ -268,8 +276,8 @@
         def begin(self):
             self.up(z, 1).start()
             self.low(z, 1).start()
-            for d in order[1:]:
-                self.across(z, d).start()
+            self.across(z, 1).start()
+            self.across(z, NX - 1).start()
 
         def relay(self, k):
             below = (z + nz - k) % nz
@@ -291,16 +299,54 @@
             def _():
                 self.low(above, k + 1).start()
 
-            for d in order[1:]:
-                self.across(below, d).start()
-
-            @pl.when(k < mid)
-            def _():
-                for d in order[1:]:
+            @pl.when(k <= self.early)
+            def _():
+                for d in (1, NX - 1):
+                    self.across(below, d).start()
+
+            @pl.when((k <= self.early) & (k < mid))
+            def _():
+                for d in (1, NX - 1):
                     self.across(above, d).start()
 
+        def late(self):
+            for k in range(self.early + 1, mid + 1):
+                for zz in ((z + nz - k) % nz, (z + k) % nz)[: 1 + (k < mid)]:
+                    for d in (1, NX - 1):
+                        self.across(zz, d).start()
+
+        def second(self, zz, d):
+            block = self.ref.at[zz, (x + NX - d) % NX, c]
+            at = (self.n * (NX - 1) + 1) * nz + zz
+            return remote(block, block, wxs_sem.at[at], wxr_sem.at[at], dev(z, (x + d) % NX, c))
+
+        def onward(self, k):
+            below = (z + nz - k) % nz
+            above = (z + k) % nz
+            both = (k > 0) & (k < mid)
+
+            @pl.when(both | (c == 0))
+            def _():
+                self.across(below, 1).wait_recv()
+                self.second(below, 1).start()
+
+            @pl.when(both | (c == 1))
+            def _():
+                self.across(above, NX - 1).wait_recv()
+                self.second(above, NX - 1).start()
+
         def gather_side(self, d):
-            if d:
+            if d == 1 or d == NX - 1:
+                for k in range(1, mid):
+                    zz = (z + k) % nz if d == 1 else (z + nz - k) % nz
+                    self.across(zz, d).wait_recv()
+
+                @pl.when(c == (1 if d == 1 else 0))
+                def _():
+                    self.across(z, d).wait_recv()
+                    self.across((z + mid) % nz, d).wait_recv()
+
+            elif d:
                 for zz in range(nz):
                     self.across(zz, d).wait_recv()
             self.side(d).start()
@@ -328,8 +374,8 @@
             for d in range(NX):
                 self.side(d).wait_send()
 
-    w_out = Weight(wo, 0)
-    w_down = Weight(wd, 1)
+    w_out = Weight(wo, 0, mid)
+    w_down = Weight(wd, 1, EARLY)
     loads[5].wait()
     w_out.begin()
 
@@ -345,16 +391,14 @@
     loads[6].wait()
 
     scale = 64 ** (-0.5) * math.log2(math.e)
-    tile = min(256, 2 * rows)
+    tile = rows
 
     def attend(blocks):
         width = len(blocks) * tokens
-
-        def body(r, carry):
-            at = pl.ds(pl.multiple_of(r * tile, tile), tile)
-            keys = jnp.concatenate([piece(slot, s)[0] for slot, s in blocks], axis=0)
-            vals = jnp.concatenate([piece(slot, s)[1] for slot, s in blocks], axis=0)
-            scores = dot_nt(qs[at, :], keys)
+        keys = jnp.concatenate([piece(slot, s)[0] for slot, s in blocks], axis=0)
+        vals = jnp.concatenate([piece(slot, s)[1] for slot, s in blocks], axis=0)
+        halves = [pl.ds(n * tile, tile) for n in range(2)]
+        for at, scores in [(at, dot_nt(qs[at, :], keys)) for at in halves]:
             old = mx[at, :]
             top = scores[:, 0:128]
             for lo in range(128, width, 128):
@@ -372,9 +416,6 @@
             acc[at, :] = acc[at, :] * factor + jnp.dot(
                 jnp.concatenate(parts, axis=1), vals, preferred_element_type=F32
             )
-            return carry
-
-        lax.fori_loop(0, 2 * rows // tile, body, 0)
 
     attend([(mine, s) for s in range(NX)])
 
@@ -400,6 +441,14 @@
         @pl.when((i % 2 == 1) & (i < 2 * mid))
         def _():
             w_out.relay((i + 1) // 2)
+
+        @pl.when((i % 2 == 1) & (i >= OUT_ON) & (i <= OUT_ON + 2 * mid))
+        def _():
+            w_out.onward((i - OUT_ON) // 2)
+
+        @pl.when((i % 2 == 0) & (i >= DOWN_ON) & (i < DOWN_ON + 2 * DOWN_N))
+        def _():
+            w_down.onward((i - DOWN_ON) // 2)
 
         @pl.when(i == DOWN_AT)
         def _():
@@ -454,6 +503,7 @@
         copy.start()
         a_copies.append(copy)
     arecv[:, my_cols] = asend[x]
+    w_down.late()
     w_out.finish_side()
     for copy in a_copies:
         copy.wait()
@@ -463,24 +513,34 @@
     hidden_width = wd.shape[4]
     feature_rows = NX * NC * wo.shape[3]
 
-    def exchange(send, recv, s_sem, r_sem):
+    cols = wo.shape[0] * feature_rows // PARTS
+    per_part = nz // PARTS
+
+    def project(rows_ref, weights, k_width, send, recv, s_sem, r_sem):
         copies = []
-        for d in range(1, n_tp):
-            to = (tp + d) % n_tp
-            copy = remote(send.at[to], recv.at[d - 1], s_sem.at[d - 1], r_sem.at[d - 1], (sp, to))
-            copy.start()
-            copies.append(copy)
+        for p in range(PARTS):
+            at = pl.ds(p * cols, cols)
+            w = weights[p * per_part : (p + 1) * per_part].reshape(cols, k_width)
+            part = dot_nt(rows_ref[...], w).astype(BF16)
+            for t in range(n_tp):
+                send[t, :, at] = part[t * n_rows : (t + 1) * n_rows, :]
+            for d in range(1, n_tp):
+                to = (tp + d) % n_tp
+                n = p * (n_tp - 1) + d - 1
+                copy = remote(
+                    send.at[to, :, at],
+                    recv.at[d - 1, :, at],
+                    s_sem.at[n],
+                    r_sem.at[n],
+                    (sp, to),
+                )
+                copy.start()
+                copies.append(copy)
         return copies
 
-    def project(i, carry):
-        at = pl.ds(pl.multiple_of(i * feature_rows, feature_rows), feature_rows)
-        part = dot_nt(arecv[...], wo[i].reshape(feature_rows, width)).astype(BF16)
-        for t in range(n_tp):
-            psend[t, :, at] = part[t * n_rows : (t + 1) * n_rows, :]
-        return carry
-
-    lax.fori_loop(0, nz, project, 0)
-    copies = exchange(psend, precv, ps_sem, pr_sem)
+    copies = project(arecv, wo, width, psend, precv, ps_sem, pr_sem)
+    for k in range(DOWN_N, EARLY + 1):
+        w_down.onward(k)
     loads[9].wait()
     total = psend[tp].astype(F32)
     for copy in copies:
@@ -495,42 +555,44 @@
     nsend[...] = normed
     my_part = pl.ds(pl.multiple_of(tp * n_rows, n_rows), n_rows)
     copies = []
-    for d in range(1, n_tp):
-        copy = remote(
-            nsend,
-            shard.at[my_part, :],
-            ns_sem.at[d - 1],
-            nr_sem.at[d - 1],
-            (sp, (tp + d) % n_tp),
-        )
-        copy.start()
-        copies.append(copy)
+    middle = nsend.shape[1] // 2
+    sides = (pl.ds(0, middle), pl.ds(middle, middle))
+    for n, side in enumerate(sides):
+        for d in range(1, n_tp):
+            copy = remote(
+                nsend.at[:, side],
+                shard.at[my_part, side],
+                ns_sem.at[n * (n_tp - 1) + d - 1],
+                nr_sem.at[n * (n_tp - 1) + d - 1],
+                (sp, (tp + d) % n_tp),
+            )
+            copy.start()
+            copies.append(copy)
     shard[my_part, :] = normed
     w_down.gather_side(0)
+    for k in range(EARLY + 1, mid + 1):
+        w_down.onward(k)
     loads[7].wait()
     loads[8].wait()
-    for copy in copies:
+    tiles = [(lo, min(lo + 256, hidden_width)) for lo in range(0, hidden_width, 256)]
+    for copy in copies[: n_tp - 1]:
         copy.wait()
-    lo = 0
-    while lo < hidden_width:
-        hi = min(lo + 256, hidden_width)
-        gate = jnp.dot(shard[...], gv[:, lo:hi], preferred_element_type=F32)
-        up = jnp.dot(shard[...], uv[:, lo:hi], preferred_element_type=F32)
+    for lo, hi in tiles:
+        left = shard[:, 0:middle]
+        gacc[:, lo:hi] = jnp.dot(left, gv[0:middle, lo:hi], preferred_element_type=F32)
+        uacc[:, lo:hi] = jnp.dot(left, uv[0:middle, lo:hi], preferred_element_type=F32)
+    for copy in copies[n_tp - 1 :]:
+        copy.wait()
+    for lo, hi in tiles:
+        left = shard[:, middle:]
+        gate = gacc[:, lo:hi] + jnp.dot(left, gv[middle:, lo:hi], preferred_element_type=F32)
+        up = uacc[:, lo:hi] + jnp.dot(left, uv[middle:, lo:hi], preferred_element_type=F32)
         hid[:, lo:hi] = (gate / (1.0 + jnp.exp(-gate)) * up).astype(BF16)
-        lo = hi
     for d in order[1:]:
         w_down.gather_side(d)
     w_down.finish_side()
 
-    def down(i, carry):
-        at = pl.ds(pl.multiple_of(i * feature_rows, feature_rows), feature_rows)
-        part = dot_nt(hid[...], wd[i].reshape(feature_rows, hidden_width)).astype(BF16)
-        for t in range(n_tp):
-            dsend[t, :, at] = part[t * n_rows : (t + 1) * n_rows, :]
-        return carry
-
-    lax.fori_loop(0, nz, down, 0)
-    copies = exchange(dsend, drecv, fs_sem, fr_sem)
+    copies = project(hid, wd, hidden_width, dsend, drecv, fs_sem, fr_sem)
 
     for d in range(1, NX):
         x_copies[d].wait_send()
@@ -598,6 +660,8 @@
             pltpu.VMEM((n_rows, features), BF16),
             pltpu.VMEM((n_rows, features), BF16),
             pltpu.VMEM((tokens, features), BF16),
+            pltpu.VMEM((tokens, hidden), F32),
+            pltpu.VMEM((tokens, hidden), F32),
             pltpu.VMEM((tokens, hidden), BF16),
             pltpu.VMEM((n_tp, n_rows, features), BF16),
             pltpu.VMEM((n_tp - 1, n_rows, features), BF16),
@@ -620,12 +684,12 @@
             dma((2 * (NX - 1) * nz,)),
             dma((2 * NX,)),
             dma((2 * NX,)),
-            dma((n_tp - 1,)),
-            dma((n_tp - 1,)),
-            dma((n_tp - 1,)),
-            dma((n_tp - 1,)),
-            dma((n_tp - 1,)),
-            dma((n_tp - 1,)),
+            dma((PARTS * (n_tp - 1),)),
+            dma((PARTS * (n_tp - 1),)),
+            dma((2 * (n_tp - 1),)),
+            dma((2 * (n_tp - 1),)),
+            dma((PARTS * (n_tp - 1),)),
+            dma((PARTS * (n_tp - 1),)),
         ],
         compiler_params=pltpu.CompilerParams(
             collective_id=0, has_side_effects=True, vmem_limit_bytes=62 * 2**20

time: 101 us -> 85.3 us (0.84)
  Pallas kernels: 99.2 us -> 83.5 us
    pallas_call x1, Pallas kernels: 99.2 us -> 83.5 us  [local(): pl.pallas_call(functools.partial(kernel, nz, n_tp), out_shape=jax.ShapeDt...]
where the time goes in v3:
time: 85.3 us; the launch traced here: 85.1 us
  Pallas kernels  83.5 us (98%)
  local copies, waits for them, and re-layouts  1.57 us (2%)
    pallas_call x1, Pallas kernels, local(): pl.pallas_call(functools.partial(kernel, nz, n_tp), out_shape=jax.ShapeDt...  83.5 us

profile of v3, /device:TPU:1, one launch (start us, length us, event | category | flops | bytes accessed | tf_op | source)
XLA Modules:
  0.0 85.1 jit_solution(1723176783495403097)
XLA Ops:
  0.0 83.5 %layer.1 = bf16[32,2048]{1,0:T(8,128)(2,1)} custom-call(bf16[32,2048]{1,0:T(8,128)(2,1)} %res_hbm.1, bf16[128,256]{1,0:T(8,128)(2,1)} %q1_hbm.1, bf16[128,256]{1,0:T(8,128)(2,1)} %k1_hbm.1, bf16[128,256]{1,0:T(8,128)(2,1)} %q2_hbm.1, bf16[128,256]{1,0:T(8,128)(2,1)} %k2_hbm.1, bf16[128,512]{1,0:T(8,128)(2,1)} %v_hbm.1, f32[4]{0:T(128)} %lam_ref.1, ...), custom_call_target="tpu_custom_call" | custom-call | tf_op jit(solution)/shard_map/layer/pallas_call | solution.py:632
  83.6 1.6 %copy.15 = bf16[32,2048]{1,0:T(8,128)(2,1)} copy(bf16[32,2048]{1,0:T(8,128)(2,1)} %layer.1) | data formatting | bytes 262144

commit v4 on v3

--- a/solution.py
+++ b/solution.py
@@ -12,11 +12,8 @@
 MESH = pl.DeviceIdType.MESH
 NX = 4
 NC = 2
-DOWN_AT = 4
-EARLY = 2
+DOWN_AT = 6
 OUT_ON = 5
-DOWN_ON = 10
-DOWN_N = 2
 PARTS = 4
 F32 = jnp.float32
 BF16 = jnp.bfloat16
@@ -215,6 +212,131 @@
         s = jnp.where(j < 0, 2 * (j + half) + 1, jnp.where(j >= steps - half, s + half, s))
         return ((z + d) % nz) * NC + core, s
 
+    class Weight:
+        def __init__(self, ref, n):
+            self.ref = ref
+            self.n = n
+
+        def up(self, zz, k):
+            block = self.ref.at[zz, x, c]
+            at = self.n * mid + k - 1
+            return remote(block, block, wus_sem.at[at], wur_sem.at[at], dev(z_up, x, c))
+
+        def low(self, zz, k):
+            block = self.ref.at[zz, x, c]
+            at = self.n * mid + k - 1
+            return remote(block, block, wls_sem.at[at], wlr_sem.at[at], dev(z_dn, x, c))
+
+        def across(self, zz, d):
+            block = self.ref.at[zz, x, c]
+            at = (self.n * (NX - 1) + d - 1) * nz + zz
+            return remote(block, block, wxs_sem.at[at], wxr_sem.at[at], dev(z, (x + d) % NX, c))
+
+        def side(self, d):
+            block = self.ref.at[:, (x + NX - d) % NX, c]
+            at = self.n * NX + d
+            return remote(block, block, wds_sem.at[at], wdr_sem.at[at], other)
+
+        def begin(self):
+            self.up(z, 1).start()
+            self.low(z, 1).start()
+
+        def begin_across(self):
+            self.across(z, 1).start()
+            self.across(z, NX - 1).start()
+
+        def relay(self, k):
+            below = (z + nz - k) % nz
+            above = (z + k) % nz
+
+            @pl.when((k < mid) | (c == 0))
+            def _():
+                self.up(below, k).wait_recv()
+
+            @pl.when((k < mid) | (c == 1))
+            def _():
+                self.low(above, k).wait_recv()
+
+            @pl.when((k < mid - 1) | ((k == mid - 1) & (c == 0)))
+            def _():
+                self.up(below, k + 1).start()
+
+            @pl.when((k < mid - 1) | ((k == mid - 1) & (c == 1)))
+            def _():
+                self.low(above, k + 1).start()
+
+        def spread(self, k):
+            below = (z + nz - k) % nz
+            above = (z + k) % nz
+            for d in (1, NX - 1):
+                self.across(below, d).start()
+
+            @pl.when(k < mid)
+            def _():
+                for d in (1, NX - 1):
+                    self.across(above, d).start()
+
+        def second(self, zz, d):
+            block = self.ref.at[zz, (x + NX - d) % NX, c]
+            at = (self.n * (NX - 1) + 1) * nz + zz
+            return remote(block, block, wxs_sem.at[at], wxr_sem.at[at], dev(z, (x + d) % NX, c))
+
+        def onward(self, k):
+            below = (z + nz - k) % nz
+            above = (z + k) % nz
+            both = (k > 0) & (k < mid)
+
+            @pl.when(both | (c == 0))
+            def _():
+                self.across(below, 1).wait_recv()
+                self.second(below, 1).start()
+
+            @pl.when(both | (c == 1))
+            def _():
+                self.across(above, NX - 1).wait_recv()
+                self.second(above, NX - 1).start()
+
+        def gather_side(self, d):
+            if d == 1 or d == NX - 1:
+                for k in range(1, mid):
+                    zz = (z + k) % nz if d == 1 else (z + nz - k) % nz
+                    self.across(zz, d).wait_recv()
+
+                @pl.when(c == (1 if d == 1 else 0))
+                def _():
+                    self.across(z, d).wait_recv()
+                    self.across((z + mid) % nz, d).wait_recv()
+
+            elif d:
+                for zz in range(nz):
+                    self.across(zz, d).wait_recv()
+            self.side(d).start()
+
+        def finish_side(self):
+            for d in range(NX):
+                self.side(d).wait_recv()
+
+        def finish_sends(self):
+            for k in range(1, mid):
+                self.up(z, k).wait_send()
+                self.low(z, k).wait_send()
+
+            @pl.when(c == 0)
+            def _():
+                self.up(z, mid).wait_send()
+
+            @pl.when(c == 1)
+            def _():
+                self.low(z, mid).wait_send()
+
+            for d in range(1, NX):
+                for zz in range(nz):
+                    self.across(zz, d).wait_send()
+            for d in range(NX):
+                self.side(d).wait_send()
+
+    w_out = Weight(wo, 0)
+    w_down = Weight(wd, 1)
     up_copy(mine, 0, 0).start()
     low_copy(mine, 0, 0).start()
     side_copy(mine, 0, 0).start()
@@ -247,138 +369,9 @@
         low_copy(mine, s, s).start()
         side_copy(mine, s, s).start()
 
-    class Weight:
-        def __init__(self, ref, n, early):
-            self.ref = ref
-            self.n = n
-            self.early = early
-
-        def up(self, zz, k):
-            block = self.ref.at[zz, x, c]
-            at = self.n * mid + k - 1
-            return remote(block, block, wus_sem.at[at], wur_sem.at[at], dev(z_up, x, c))
-
-        def low(self, zz, k):
-            block = self.ref.at[zz, x, c]
-            at = self.n * mid + k - 1
-            return remote(block, block, wls_sem.at[at], wlr_sem.at[at], dev(z_dn, x, c))
-
-        def across(self, zz, d):
-            block = self.ref.at[zz, x, c]
-            at = (self.n * (NX - 1) + d - 1) * nz + zz
-            return remote(block, block, wxs_sem.at[at], wxr_sem.at[at], dev(z, (x + d) % NX, c))
-
-        def side(self, d):
-            block = self.ref.at[:, (x + NX - d) % NX, c]
-            at = self.n * NX + d
-            return remote(block, block, wds_sem.at[at], wdr_sem.at[at], other)
-
-        def begin(self):
-            self.up(z, 1).start()
-            self.low(z, 1).start()
-            self.across(z, 1).start()
-            self.across(z, NX - 1).start()
-
-        def relay(self, k):
-            below = (z + nz - k) % nz
-            above = (z + k) % nz
-
-            @pl.when((k < mid) | (c == 0))
-            def _():
-                self.up(below, k).wait_recv()
-
-            @pl.when((k < mid) | (c == 1))
-            def _():
-                self.low(above, k).wait_recv()
-
-            @pl.when((k < mid - 1) | ((k == mid - 1) & (c == 0)))
-            def _():
-                self.up(below, k + 1).start()
-
-            @pl.when((k < mid - 1) | ((k == mid - 1) & (c == 1)))
-            def _():
-                self.low(above, k + 1).start()
-
-            @pl.when(k <= self.early)
-            def _():
-                for d in (1, NX - 1):
-                    self.across(below, d).start()
-
-            @pl.when((k <= self.early) & (k < mid))
-            def _():
-                for d in (1, NX - 1):
-                    self.across(above, d).start()
-
-        def late(self):
-            for k in range(self.early + 1, mid + 1):
-                for zz in ((z + nz - k) % nz, (z + k) % nz)[: 1 + (k < mid)]:
-                    for d in (1, NX - 1):
-                        self.across(zz, d).start()
-
-        def second(self, zz, d):
-            block = self.ref.at[zz, (x + NX - d) % NX, c]
-            at = (self.n * (NX - 1) + 1) * nz + zz
-            return remote(block, block, wxs_sem.at[at], wxr_sem.at[at], dev(z, (x + d) % NX, c))
-
-        def onward(self, k):
-            below = (z + nz - k) % nz
-            above = (z + k) % nz
-            both = (k > 0) & (k < mid)
-
-            @pl.when(both | (c == 0))
-            def _():
-                self.across(below, 1).wait_recv()
-                self.second(below, 1).start()
-
-            @pl.when(both | (c == 1))
-            def _():
-                self.across(above, NX - 1).wait_recv()
-                self.second(above, NX - 1).start()
-
-        def gather_side(self, d):
-            if d == 1 or d == NX - 1:
-                for k in range(1, mid):
-                    zz = (z + k) % nz if d == 1 else (z + nz - k) % nz
-                    self.across(zz, d).wait_recv()
-
-                @pl.when(c == (1 if d == 1 else 0))
-                def _():
-                    self.across(z, d).wait_recv()
-                    self.across((z + mid) % nz, d).wait_recv()
-
-            elif d:
-                for zz in range(nz):
-                    self.across(zz, d).wait_recv()
-            self.side(d).start()
-
-        def finish_side(self):
-            for d in range(NX):
-                self.side(d).wait_recv()
-
-        def finish_sends(self):
-            for k in range(1, mid):
-                self.up(z, k).wait_send()
-                self.low(z, k).wait_send()
-
-            @pl.when(c == 0)
-            def _():
-                self.up(z, mid).wait_send()
-
-            @pl.when(c == 1)
-            def _():
-                self.low(z, mid).wait_send()
-
-            for d in range(1, NX):
-                for zz in range(nz):
-                    self.across(zz, d).wait_send()
-            for d in range(NX):
-                self.side(d).wait_send()
-
-    w_out = Weight(wo, 0, mid)
-    w_down = Weight(wd, 1, EARLY)
     loads[5].wait()
     w_out.begin()
-
+    w_out.begin_across()
     acc[...] = jnp.zeros_like(acc)
     tot[...] = jnp.zeros_like(tot)
     mx[...] = jnp.full(mx.shape, -3e38, F32)
@@ -424,6 +417,15 @@
         above, above_s = from_above(i, c)
         up_copy(below, below_s, i).wait_recv()
 
+        @pl.when(i == DOWN_AT)
+        def _():
+            w_down.begin()
+
+        @pl.when((i > DOWN_AT) & ((i - DOWN_AT) % NX == 0))
+        def _():
+            w_down.relay((i - DOWN_AT) // NX)
+            w_down.spread((i - DOWN_AT) // NX)
+
         @pl.when(i < steps - NX)
         def _():
             up_copy(below, below_s, i + NX).start()
@@ -438,25 +440,22 @@
         side_copy(below, below_s, NX + i).start()
         side_copy(above, above_s, NX + steps + i).start()
 
+        @pl.when(i == DOWN_AT)
+        def _():
+            w_down.begin_across()
+
         @pl.when((i % 2 == 1) & (i < 2 * mid))
         def _():
             w_out.relay((i + 1) // 2)
-
-        @pl.when((i % 2 == 1) & (i >= OUT_ON) & (i <= OUT_ON + 2 * mid))
+            w_out.spread((i + 1) // 2)
+
+        @pl.when((i % 2 == 1) & (i >= OUT_ON))
         def _():
             w_out.onward((i - OUT_ON) // 2)
 
-        @pl.when((i % 2 == 0) & (i >= DOWN_ON) & (i < DOWN_ON + 2 * DOWN_N))
+        @pl.when((i > DOWN_AT) & ((i - DOWN_AT) % NX == 1) & (i >= DOWN_AT + NX))
         def _():
-            w_down.onward((i - DOWN_ON) // 2)
-
-        @pl.when(i == DOWN_AT)
-        def _():
-            w_down.begin()
-
-        @pl.when((i % 2 == 0) & (i > DOWN_AT) & (i <= DOWN_AT + 2 * mid))
-        def _():
-            w_down.relay((i - DOWN_AT) // 2)
+            w_down.onward((i - DOWN_AT) // NX - 1)
 
         other_b, other_bs = from_below(i - half, 1 - c)
         other_a, other_as = from_above(i - half, 1 - c)
@@ -468,7 +467,14 @@
         return carry
 
     lax.fori_loop(0, steps, step, 0)
+    in_loop = (steps - 1 - DOWN_AT) // NX
     w_out.gather_side(0)
+    for k in range((steps - 1 - steps % 2 - OUT_ON) // 2 + 1, mid + 1):
+        w_out.onward(k)
+    for k in range((steps - 2 - DOWN_AT) // NX, in_loop):
+        w_down.onward(k)
+    if in_loop < mid - 1:
+        w_down.relay(in_loop + 1)
     last = []
     for j in range(steps - half, steps):
         b = from_below(j, 1 - c)
@@ -503,7 +509,8 @@
         copy.start()
         a_copies.append(copy)
     arecv[:, my_cols] = asend[x]
-    w_down.late()
+    if in_loop < mid - 1:
+        w_down.spread(in_loop + 1)
     w_out.finish_side()
     for copy in a_copies:
         copy.wait()
@@ -539,7 +546,10 @@
         return copies
 
     copies = project(arecv, wo, width, psend, precv, ps_sem, pr_sem)
-    for k in range(DOWN_N, EARLY + 1):
+    for k in range(min(in_loop + 2, mid), mid + 1):
+        w_down.relay(k)
+        w_down.spread(k)
+    for k in range(in_loop, mid):
         w_down.onward(k)
     loads[9].wait()
     total = psend[tp].astype(F32)
@@ -570,8 +580,7 @@
             copies.append(copy)
     shard[my_part, :] = normed
     w_down.gather_side(0)
-    for k in range(EARLY + 1, mid + 1):
-        w_down.onward(k)
+    w_down.onward(mid)
     loads[7].wait()
     loads[8].wait()
     tiles = [(lo, min(lo + 256, hidden_width)) for lo in range(0, hidden_width, 256)]
@@ -583,12 +592,14 @@
         uacc[:, lo:hi] = jnp.dot(left, uv[0:middle, lo:hi], preferred_element_type=F32)
     for copy in copies[n_tp - 1 :]:
         copy.wait()
+    w_down.gather_side(1)
+    w_down.gather_side(NX - 1)
     for lo, hi in tiles:
         left = shard[:, middle:]
         gate = gacc[:, lo:hi] + jnp.dot(left, gv[middle:, lo:hi], preferred_element_type=F32)
         up = uacc[:, lo:hi] + jnp.dot(left, uv[middle:, lo:hi], preferred_element_type=F32)
         hid[:, lo:hi] = (gate / (1.0 + jnp.exp(-gate)) * up).astype(BF16)
-    for d in order[1:]:
+    for d in range(2, NX - 1):
         w_down.gather_side(d)
     w_down.finish_side()
 

time: 85.3 us -> 79.1 us (0.927)
  Pallas kernels: 83.5 us -> 77.4 us
    pallas_call x1, Pallas kernels: 83.5 us -> 77.4 us  [local(): pl.pallas_call(functools.partial(kernel, nz, n_tp), out_shape=jax.ShapeDt...]
where the time goes in v4:
time: 79.1 us; the launch traced here: 79 us
  Pallas kernels  77.4 us (98%)
  local copies, waits for them, and re-layouts  1.57 us (2%)
    pallas_call x1, Pallas kernels, local(): pl.pallas_call(functools.partial(kernel, nz, n_tp), out_shape=jax.ShapeDt...  77.4 us

profile of v4, /device:TPU:1, one launch (start us, length us, event | category | flops | bytes accessed | tf_op | source)
XLA Modules:
  0.0 79.0 jit_solution(6926940643202458235)
XLA Ops:
  0.0 77.4 %layer.1 = bf16[32,2048]{1,0:T(8,128)(2,1)} custom-call(bf16[32,2048]{1,0:T(8,128)(2,1)} %res_hbm.1, bf16[128,256]{1,0:T(8,128)(2,1)} %q1_hbm.1, bf16[128,256]{1,0:T(8,128)(2,1)} %k1_hbm.1, bf16[128,256]{1,0:T(8,128)(2,1)} %q2_hbm.1, bf16[128,256]{1,0:T(8,128)(2,1)} %k2_hbm.1, bf16[128,512]{1,0:T(8,128)(2,1)} %v_hbm.1, f32[4]{0:T(128)} %lam_ref.1, ...), custom_call_target="tpu_custom_call" | custom-call | tf_op jit(solution)/shard_map/layer/pallas_call | solution.py:643
  77.4 1.6 %copy.15 = bf16[32,2048]{1,0:T(8,128)(2,1)} copy(bf16[32,2048]{1,0:T(8,128)(2,1)} %layer.1) | data formatting | bytes 262144

commit v5 on v4

--- a/solution.py
+++ b/solution.py
@@ -14,7 +14,7 @@
 NC = 2
 DOWN_AT = 6
 OUT_ON = 5
-PARTS = 4
+PARTS = 2
 F32 = jnp.float32
 BF16 = jnp.bfloat16
 
@@ -440,7 +440,7 @@
         side_copy(below, below_s, NX + i).start()
         side_copy(above, above_s, NX + steps + i).start()
 
-        @pl.when(i == DOWN_AT)
+        @pl.when(i == 3)
         def _():
             w_down.begin_across()
 
@@ -586,14 +586,14 @@
     tiles = [(lo, min(lo + 256, hidden_width)) for lo in range(0, hidden_width, 256)]
     for copy in copies[: n_tp - 1]:
         copy.wait()
+    w_down.gather_side(1)
+    w_down.gather_side(NX - 1)
     for lo, hi in tiles:
         left = shard[:, 0:middle]
         gacc[:, lo:hi] = jnp.dot(left, gv[0:middle, lo:hi], preferred_element_type=F32)
         uacc[:, lo:hi] = jnp.dot(left, uv[0:middle, lo:hi], preferred_element_type=F32)
     for copy in copies[n_tp - 1 :]:
         copy.wait()
-    w_down.gather_side(1)
-    w_down.gather_side(NX - 1)
     for lo, hi in tiles:
         left = shard[:, middle:]
         gate = gacc[:, lo:hi] + jnp.dot(left, gv[middle:, lo:hi], preferred_element_type=F32)

time: 79.1 us -> 79.1 us (level)
  no operation moved by 1% of the time
where the time goes in v5:
time: 79.1 us; the launch traced here: 79 us
  Pallas kernels  77.4 us (98%)
  local copies, waits for them, and re-layouts  1.57 us (2%)
    pallas_call x1, Pallas kernels, local(): pl.pallas_call(functools.partial(kernel, nz, n_tp), out_shape=jax.ShapeDt...  77.4 us

profile of v5, /device:TPU:1, one launch (start us, length us, event | category | flops | bytes accessed | tf_op | source)
XLA Modules:
  0.0 79.0 jit_solution(16430921608833726510)
XLA Ops:
  0.0 77.4 %layer.1 = bf16[32,2048]{1,0:T(8,128)(2,1)} custom-call(bf16[32,2048]{1,0:T(8,128)(2,1)} %res_hbm.1, bf16[128,256]{1,0:T(8,128)(2,1)} %q1_hbm.1, bf16[128,256]{1,0:T(8,128)(2,1)} %k1_hbm.1, bf16[128,256]{1,0:T(8,128)(2,1)} %q2_hbm.1, bf16[128,256]{1,0:T(8,128)(2,1)} %k2_hbm.1, bf16[128,512]{1,0:T(8,128)(2,1)} %v_hbm.1, f32[4]{0:T(128)} %lam_ref.1, ...), custom_call_target="tpu_custom_call" | custom-call | tf_op jit(solution)/shard_map/layer/pallas_call | solution.py:643
  77.4 1.6 %copy.15 = bf16[32,2048]{1,0:T(8,128)(2,1)} copy(bf16[32,2048]{1,0:T(8,128)(2,1)} %layer.1) | data formatting | bytes 262144

commit v6 on v4

--- a/solution.py
+++ b/solution.py
@@ -248,6 +248,7 @@
         def relay(self, k):
             below = (z + nz - k) % nz
             above = (z + k) % nz
+            after_k = jnp.minimum(k + 1, mid)
 
             @pl.when((k < mid) | (c == 0))
             def _():
@@ -259,11 +260,11 @@
 
             @pl.when((k < mid - 1) | ((k == mid - 1) & (c == 0)))
             def _():
-                self.up(below, k + 1).start()
+                self.up(below, after_k).start()
 
             @pl.when((k < mid - 1) | ((k == mid - 1) & (c == 1)))
             def _():
-                self.low(above, k + 1).start()
+                self.low(above, after_k).start()
 
         def spread(self, k):
             below = (z + nz - k) % nz

time: 79.1 us -> 79.2 us (level)
  no operation moved by 1% of the time
where the time goes in v6:
time: 79.2 us; the launch traced here: 79 us
  Pallas kernels  77.4 us (98%)
  local copies, waits for them, and re-layouts  1.57 us (2%)
    pallas_call x1, Pallas kernels, local(): pl.pallas_call(functools.partial(kernel, nz, n_tp), out_shape=jax.ShapeDt...  77.4 us

profile of v6, /device:TPU:1, one launch (start us, length us, event | category | flops | bytes accessed | tf_op | source)
XLA Modules:
  0.0 79.0 jit_solution(14734741197657239668)
XLA Ops:
  0.0 77.4 %layer.1 = bf16[32,2048]{1,0:T(8,128)(2,1)} custom-call(bf16[32,2048]{1,0:T(8,128)(2,1)} %res_hbm.1, bf16[128,256]{1,0:T(8,128)(2,1)} %q1_hbm.1, bf16[128,256]{1,0:T(8,128)(2,1)} %k1_hbm.1, bf16[128,256]{1,0:T(8,128)(2,1)} %q2_hbm.1, bf16[128,256]{1,0:T(8,128)(2,1)} %k2_hbm.1, bf16[128,512]{1,0:T(8,128)(2,1)} %v_hbm.1, f32[4]{0:T(128)} %lam_ref.1, ...), custom_call_target="tpu_custom_call" | custom-call | tf_op jit(solution)/shard_map/layer/pallas_call | solution.py:644
  77.4 1.6 %copy.15 = bf16[32,2048]{1,0:T(8,128)(2,1)} copy(bf16[32,2048]{1,0:T(8,128)(2,1)} %layer.1) | data formatting | bytes 262144
